TPU v7x, 32 devices: a whole 2x2x4 slice. The times are simulated.
32 devices in a mesh: grp: 2 (over x), sp: 4 (over y, core), tp: 4 (over z).
Axes of the slice: x: 2, y: 2, z: 4, core: 2. Of those that a mesh axis runs over, the one named last changes fastest.
Arguments:
- resid_in: bfloat16 [4096, 2048], P(('grp', 'sp', 'tp')), parts along dimension 0, may hold values from -6 to 6
- pool_input: bfloat16 [4096, 1024], P(('grp', 'sp'), 'tp'), parts along dimension 0, may hold values from -6 to 6
- pool_weight: bfloat16 [4, 256, 256], replicated, may hold values from -0.375 to 0.375
- pool_scale: float32 [1024], replicated, may hold values from 0.2 to 0.8
- out_weight: bfloat16 [1024, 2048], replicated, may hold values from -0.1875 to 0.1875
- mix_gain: float32 [2048], replicated, may hold values from 0.1 to 1.9
- ffn_gain: float32 [2048], replicated, may hold values from 0.1 to 1.9
- w_gate: bfloat16 [32, 2048, 1024], P('sp', None, 'tp'), may hold values from -0.375 to 0.375
- w_up: bfloat16 [32, 2048, 1024], P('sp', None, 'tp'), may hold values from -0.375 to 0.375
- w_down: bfloat16 [32, 1024, 2048], P('sp', 'tp'), may hold values from -0.1875 to 0.1875
- routes: int32 [4096, 2], P(('grp', 'sp', 'tp')), parts along dimension 0, may hold values from 0 to 31, all different within a row; in each aligned block of 128 rows (0 to 127, 128 to 255, ...) at most 9 rows name the same one
- route_weight: float32 [4096, 2], P(('grp', 'sp', 'tp')), parts along dimension 0, may hold values from 0.1 to 1
- post_gain: float32 [2048], replicated, may hold values from 0.1 to 1.9
Outputs:
- layer_out: bfloat16 [4096, 2048], P(('grp', 'sp', 'tp')), parts along dimension 0
There are 2 independent parts, one for each index of `grp`. A program takes and returns all parts, laid end to end along the dimension named above; an argument that names none is the same for every part. Nothing has to cross between parts.
Inputs may be any that keep to these rules, and one draw needn't show every extreme that they name: `routes`: each row names 2 different experts. The rows of one device name any one expert at most 9 times, and in every draw some device's rows name some expert exactly 9 times.
All inputs are finite; a program needn't handle non-finite values.
Results may differ from a plain program's by a relative error of at most 0.011.
Values may be sent and summed in bfloat16 or wider, within the bound.
A program may use at most 128 MiB of HBM per device.

v0:
```python
import jax
import jax.numpy as jnp
from jax import lax
from jax.sharding import PartitionSpec as P

GROUPS = 4
GROUP_DIM = 256
TOP = 2
CAP = 9


pool_windows = (2, 4, 8, 16)
reach_back = 15
norm_eps = 1e-06
clamp_limit = 7.0
glu_alpha = 1.702


def passed_along(x, axis, by):
    size = lax.axis_size(axis)
    pairs = [(i, i + by) for i in range(size) if 0 <= i + by < size]
    return lax.ppermute(x, axis, pairs)


def rms_scale(values, gain_vec):
    inverse = lax.rsqrt(jnp.mean(values * values, axis=-1, keepdims=True) + norm_eps)
    return values * inverse * gain_vec


def clamped_unit(gate_pre, upward):
    gate_clip = jnp.minimum(gate_pre, clamp_limit)
    linear = jnp.clip(upward, -clamp_limit, clamp_limit)
    return gate_clip * jax.nn.sigmoid(glu_alpha * gate_clip) * (linear + 1.0)


def per_device(
    resid_in,
    pool_input,
    pool_weight,
    pool_scale,
    out_weight,
    mix_gain,
    ffn_gain,
    w_gate,
    w_up,
    w_down,
    routes,
    route_weight,
    post_gain,
):
    n_sp = lax.axis_size("sp")
    n_tp = lax.axis_size("tp")
    seg_rows, channels = pool_input.shape
    last_rows = pool_input[seg_rows - reach_back :]
    before = passed_along(last_rows, "sp", 1)
    extended = jnp.concatenate([before, pool_input], axis=0).astype(jnp.float32)
    first_chan = lax.axis_index("tp") * channels
    chan_group = (first_chan + lax.iota(jnp.int32, channels)) // GROUP_DIM
    positions = lax.axis_index("sp") * seg_rows + lax.iota(jnp.int32, seg_rows)
    window = jnp.zeros((channels,), jnp.int32)
    for group_level, win_len in enumerate(pool_windows):
        window = jnp.where(chan_group == group_level, win_len, window)
    running = jnp.zeros((seg_rows, channels), jnp.float32)
    window_sum = running
    for offset in range(pool_windows[-1]):
        running = running + extended[reach_back - offset : reach_back - offset + seg_rows]
        if offset + 1 in pool_windows:
            window_sum = jnp.where(window[None, :] == offset + 1, running, window_sum)
    divisor = jnp.minimum(positions[:, None] + 1, window[None, :]).astype(jnp.float32)
    mixed_rows = (window_sum / divisor - extended[reach_back:]).astype(jnp.bfloat16)
    token_mixed = lax.all_to_all(mixed_rows, "tp", split_axis=0, concat_axis=1, tiled=True)
    tok_rows = token_mixed.shape[0]
    pooled = jnp.einsum(
        "tgc,gcd->tgd",
        token_mixed.reshape(tok_rows, GROUPS, GROUP_DIM),
        pool_weight,
        preferred_element_type=jnp.float32,
    )
    pooled = (
        (pooled * pool_scale.reshape(GROUPS, GROUP_DIM)).astype(jnp.bfloat16).reshape(tok_rows, -1)
    )
    mix_out = jnp.dot(pooled, out_weight, preferred_element_type=jnp.float32)
    residual = (resid_in.astype(jnp.float32) + rms_scale(mix_out, mix_gain)).astype(jnp.bfloat16)
    normed = rms_scale(residual.astype(jnp.float32), ffn_gain).astype(jnp.bfloat16)
    width = normed.shape[1]
    local_experts = w_gate.shape[0]
    n_experts = local_experts * n_sp
    slot_total = n_experts * CAP
    flat_route = routes.reshape(-1)
    onehot = (flat_route[:, None] == lax.iota(jnp.int32, n_experts)[None, :]).astype(jnp.int32)
    slot_rank = jnp.sum((jnp.cumsum(onehot, axis=0) - onehot) * onehot, axis=1)
    slot_index = flat_route * CAP + slot_rank
    picker = slot_index[:, None] == lax.iota(jnp.int32, slot_total)[None, :]
    picker_rows = picker.astype(jnp.bfloat16)
    token_pick = jnp.sum(
        picker.reshape(tok_rows, TOP, slot_total).astype(jnp.float32), axis=1
    ).astype(jnp.bfloat16)
    buffer = lax.dot_general(
        token_pick, normed, (((0,), (0,)), ((), ())), preferred_element_type=jnp.float32
    )
    outgoing = buffer.astype(jnp.bfloat16).reshape(n_sp, local_experts * CAP, width)
    at_owner = lax.all_to_all(outgoing, "sp", split_axis=0, concat_axis=0, tiled=True)
    arrived = lax.all_gather(at_owner[:, None], "tp", axis=1, tiled=True)
    arrived = arrived.reshape(n_sp, n_tp, local_experts, CAP, width)
    gate_pre = jnp.einsum("sklcd,ldf->sklcf", arrived, w_gate, preferred_element_type=jnp.float32)
    upward = jnp.einsum("sklcd,ldf->sklcf", arrived, w_up, preferred_element_type=jnp.float32)
    activated = clamped_unit(gate_pre, upward).astype(jnp.bfloat16)
    terms = jnp.einsum("sklcf,lfd->kslcd", activated, w_down, preferred_element_type=jnp.float32)
    summed = lax.psum_scatter(
        terms.reshape(1 * lax.axis_size("tp"), n_sp, local_experts * CAP, width).astype(
            jnp.bfloat16
        ),
        "tp",
        scatter_dimension=0,
        tiled=True,
    ).astype(jnp.float32)
    results = summed[0].astype(jnp.bfloat16)
    returned = lax.all_to_all(results, "sp", split_axis=0, concat_axis=0, tiled=True).reshape(
        slot_total, width
    )
    gathered = jnp.dot(picker_rows, returned, preferred_element_type=jnp.float32)
    expert_mix = jnp.sum(gathered.reshape(tok_rows, TOP, width) * route_weight[:, :, None], axis=1)
    return (residual.astype(jnp.float32) + rms_scale(expert_mix, post_gain)).astype(jnp.bfloat16)


def solution(mesh):
    in_specs = (
        P(("grp", "sp", "tp"), None),
        P(("grp", "sp"), "tp"),
        P(),
        P(),
        P(),
        P(),
        P(),
        P("sp", None, "tp"),
        P("sp", None, "tp"),
        P("sp", "tp", None),
        P(("grp", "sp", "tp"), None),
        P(("grp", "sp", "tp"), None),
        P(),
    )
    out_specs = P(("grp", "sp", "tp"), None)
    return jax.shard_map(
        per_device, mesh=mesh, in_specs=in_specs, out_specs=out_specs, check_vma=False
    )
```

profile of v0, /device:TPU:0, one launch (start us, length us, event | category | flops | bytes accessed | tf_op | source)
XLA Modules:
  0.0 289.7 jit_solution(11698675400046572136)
XLA Ops:
  6.5 0.0 copy-start
  6.5 0.8 slice.58
  7.3 2.4 collective-permute-start
  9.8 0.8 copy.52
  10.5 0.1 eq.194
  10.7 0.6 reduce-window.6
  11.3 0.2 slice_reduce_fusion
  11.5 0.1 eq.190
  11.7 0.0 collective-permute-done
  11.7 1.0 maximum_convert_fusion
  12.7 0.0 copy-start.6
  12.7 0.0 copy-start.5
  12.7 1.5 fusion.36
  14.2 5.7 %all-to-all-start = ((bf16[4,128,256]{2,1,0:T(8,128)(2,1)}), bf16[4,128,256]{2,1,0:T(8,128)(2,1)S(1)}, u32[]{:S(2)}, u32[]{:S(2)}) async-start(bf16[4,128,256]{2,1,0:T(8,128)(2,1)} %bitcast), calls=%async_computation | async-start | bytes 524288 | tf_op jit(solution)/shard_map/all_to_all | solution.py:71
  19.9 0.0 all-gather.3.cloned.1.call-start
  19.9 0.1 fusion.44
  20.0 0.0 copy-done.6
  20.0 0.1 reduce_sum.58
  20.1 0.1 copy.55
  20.2 0.0 copy-done.5
  20.2 0.1 convert_reduce_fusion
  20.3 8.4 %all-to-all-done = bf16[4,128,256]{2,1,0:T(8,128)(2,1)S(1)} async-done(((bf16[4,128,256]{2,1,0:T(8,128)(2,1)}), bf16[4,128,256]{2,1,0:T(8,128)(2,1)S(1)}, u32[]{:S(2)}, u32[]{:S(2)}) %all-to-all-start) | async-done | bytes 262176 | tf_op jit(solution)/shard_map/all_to_all | solution.py:71
  28.7 0.0 copy-done
  28.7 0.2 fusion.21
  29.0 0.2 copy.51
  29.1 0.0 copy-start.1
  29.2 0.0 copy-start.2
  29.2 0.0 copy-start.3
  29.2 3.1 %multiply_reduce_fusion.1 = (f32[128]{0:T(128)S(1)}, f32[128,2048]{1,0:T(8,128)S(1)}) fusion(bf16[128,1024]{0,1:T(8,128)(2,1)S(1)} %bitcast.91, bf16[1024,2048]{1,0:T(8,128)(2,1)} %param.17), kind=kOutput, calls=%fused_computation.32 | convolution fusion | flops 537395072 | bytes 5505536 | tf_op jit(solution)/shard_map/dot_general | solution.py:82
  32.3 0.0 copy-done.1
  32.3 0.0 copy-done.2
  32.3 0.4 fusion.22
  32.7 0.0 copy-done.3
  32.7 0.6 convolution_convert_fusion
  33.2 18.3 %all_to_all.26 = bf16[4,72,2048]{2,1,0:T(8,128)(2,1)S(1)} all-to-all(bf16[4,72,2048]{2,1,0:T(8,128)(2,1)S(1)} %bitcast.88), channel_id=1, replica_groups=mesh['grp'=2,'sp'=4,'tp'=4] {'sp'}, dimensions={0} | all-to-all | bytes 2359296 | tf_op jit(solution)/shard_map/all_to_all | solution.py:102
  51.5 1.9 copy.56
  53.4 0.0 all-gather.3.cloned.1.call-update
  53.4 0.0 reduce-scatter.2.cloned.1.call-start
  53.5 88.8 %all-gather.3.cloned.1.call-done = bf16[4,288,2048]{2,0,1:T(4,128)(2,1)} async-done(((bf16[4,72,2048]{2,0,1:T(4,128)(2,1)}), bf16[4,288,2048]{2,0,1:T(4,128)(2,1)}) %all-gather.3.cloned.1.call-update) | async-done | bytes 4718608 | tf_op jit(solution)/shard_map/all_gather | solution.py:103
  142.3 8.4 %fusion = f32[8,4,4,9,256]{4,3,2,1,0:T(8,128)S(1)} fusion(bf16[4,4,8,9,2048]{4,0,3,2,1:T(4,128)(2,1)} %bitcast.92, bf16[8,2048,256]{2,1,0:T(8,128)(2,1)} %param.21), kind=kOutput, calls=%fused_computation | convolution fusion | flops 1207959552 | bytes 14286848 | tf_op jit(solution)/shard_map/sklcd,ldf->sklcf/dot_general | solution.py:106
  150.7 14.0 %convert_bitcast_fusion = bf16[4,4,8,9,2048]{4,3,0,1,2:T(8,128)(2,1)} fusion(bf16[8,256,2048]{2,1,0:T(8,128)(2,1)} %param.22, f32[8,4,4,9,256]{4,3,2,1,0:T(8,128)S(1)} %fusion, bf16[8,2048,256]{2,1,0:T(8,128)(2,1)} %param.20, bf16[4,4,8,9,2048]{4,0,3,2,1:T(4,128)(2,1)} %bitcast.93), kind=kOutput, calls=%fused_computation.8 | convolution fusion | flops 2421227520 | bytes 27394048 | tf_op jit(solution)/shard_map/sklcf,lfd->kslcd/dot_general | solution.py:108
  164.7 8.3 %copy.59 = bf16[4,4,8,9,2048]{4,1,3,2,0:T(4,128)(2,1)S(1)} copy(bf16[4,4,8,9,2048]{4,3,0,1,2:T(8,128)(2,1)} %convert_bitcast_fusion) | data formatting | bytes 9437184 | tf_op jit(solution)/shard_map/convert_element_type | solution.py:110
  173.0 4.7 %copy.60 = bf16[4,4,72,2048]{3,2,1,0:T(8,128)(2,1)} copy(bf16[4,4,72,2048]{3,1,2,0:T(4,128)(2,1)S(1)} %bitcast.87) | data formatting | bytes 9437184 | tf_op jit(solution)/shard_map/convert_element_type | solution.py:110
  177.7 0.0 reduce-scatter.2.cloned.1.call-update
  177.8 0.0 copy-start.7
  177.8 83.8 %reduce-scatter.2.cloned.1.call-done = bf16[1,4,72,2048]{3,2,1,0:T(8,128)(2,1)} async-done(((bf16[4,4,72,2048]{3,2,1,0:T(8,128)(2,1)}), bf16[1,4,72,2048]{3,2,1,0:T(8,128)(2,1)}) %reduce-scatter.2.cloned.1.call-update) | async-done | bytes 1179664 | tf_op jit(solution)/shard_map/reduce_scatter | solution.py:109
  261.6 19.3 %all_to_all.27 = bf16[4,72,2048]{2,1,0:T(8,128)(2,1)S(1)} all-to-all(bf16[4,72,2048]{2,1,0:T(8,128)(2,1)} %bitcast.89), channel_id=1, replica_groups=mesh['grp'=2,'sp'=4,'tp'=4] {'sp'}, dimensions={0} | all-to-all | bytes 2359296 | tf_op jit(solution)/shard_map/all_to_all | solution.py:118
  280.9 0.0 copy-start.4
  280.9 0.0 copy-done.7
  280.9 0.8 fusion.15
  281.7 0.2 multiply_reduce_fusion
  281.9 0.0 copy-done.4
  281.9 1.0 fusion.25
  (12 shorter events, 0.1 us)
Async XLA Ops:
  6.5 22.2 %copy-start = (bf16[4,256,256]{2,1,0:T(8,128)(2,1)S(1)}, bf16[4,256,256]{2,1,0:T(8,128)(2,1)}, u32[]{:S(2)}) copy-start(bf16[4,256,256]{2,1,0:T(8,128)(2,1)} %param.15) | copy-start | bytes 1572868
  7.3 4.4 %collective-permute-start = (bf16[15,256]{1,0:T(8,128)(2,1)S(1)}, bf16[15,256]{1,0:T(8,128)(2,1)S(1)}, u32[]{:S(2)}, u32[]{:S(2)}) collective-permute-start(bf16[15,256]{1,0:T(8,128)(2,1)S(1)} %slice.58), channel_id=1, source_target_pairs={{0,4},{4,8},{8,12},{1,5},{5,9},{9,13},{2,6},{6,10},{10,14},{3,7},{... | collective-permute-start | bytes 23048 | tf_op jit(solution)/shard_map/ppermute | solution.py:22
  12.7 7.3 %copy-start.6 = (f32[1024]{0:T(1024)S(1)}, f32[1024]{0:T(1024)}, u32[]{:S(2)}) copy-start(f32[1024]{0:T(1024)} %param.16) | copy-start | bytes 12292
  12.7 7.5 %copy-start.5 = (s32[128,2]{0,1:T(2,128)S(1)}, s32[128,2]{0,1:T(2,128)}, u32[]{:S(2)}) copy-start(s32[128,2]{0,1:T(2,128)} %param.23) | copy-start | bytes 3076
  14.2 14.5 %all-to-all-start = ((bf16[4,128,256]{2,1,0:T(8,128)(2,1)}), bf16[4,128,256]{2,1,0:T(8,128)(2,1)S(1)}, u32[]{:S(2)}, u32[]{:S(2)}) async-start(bf16[4,128,256]{2,1,0:T(8,128)(2,1)} %bitcast), calls=%async_computation | async-start | bytes 524288 | tf_op jit(solution)/shard_map/all_to_all | solution.py:71
  19.9 122.4 %all-gather.3.cloned.1.call-start = ((), (), s32[]{:S(2)}) async-start(), calls=%async_computation.5 | async-start | bytes 5898240 | tf_op jit(solution)/shard_map/all_gather | solution.py:103
  29.1 3.1 %copy-start.1 = (bf16[128,2048]{1,0:T(8,128)(2,1)S(1)}, bf16[128,2048]{1,0:T(8,128)(2,1)}, u32[]{:S(2)}) copy-start(bf16[128,2048]{1,0:T(8,128)(2,1)} %param.13) | copy-start | bytes 1572868
  29.2 3.1 %copy-start.2 = (f32[2048]{0:T(1024)S(1)}, f32[2048]{0:T(1024)}, u32[]{:S(2)}) copy-start(f32[2048]{0:T(1024)} %param.18) | copy-start | bytes 24580
  29.2 3.5 %copy-start.3 = (f32[2048]{0:T(1024)S(1)}, f32[2048]{0:T(1024)}, u32[]{:S(2)}) copy-start(f32[2048]{0:T(1024)} %param.19) | copy-start | bytes 24580
  53.4 208.1 %reduce-scatter.2.cloned.1.call-start = ((), (), s32[]{:S(2)}) async-start(), calls=%async_computation.4 | async-start | bytes 5898240 | tf_op jit(solution)/shard_map/reduce_scatter | solution.py:109
  177.8 103.2 %copy-start.7 = (f32[128,2]{0,1:T(2,128)S(1)}, f32[128,2]{0,1:T(2,128)}, u32[]{:S(2)}) copy-start(f32[128,2]{0,1:T(2,128)} %param.24) | copy-start | bytes 3076
  280.9 0.9 copy-start.4
Sparse Core Ops, SparseCore 0:
  53.6 88.7 all-gather.2
  177.9 83.6 reduce-scatter.1
where the time goes:
time: 290 us
  waiting for transfers between devices  181 us (62%)
  blocking collectives  37.6 us (13%)
  matrix products  27 us (9%)
  local copies, waits for them, and re-layouts  17.3 us (6%)
  between operations  13.6 us (5%)
  starting transfers between devices  8.12 us (3%)
  other arithmetic  4.92 us (2%)
    all_gather x1, waiting for transfers between devices, per_device(): arrived = lax.all_gather(at_owner[:, None], 'tp', axis=1, tiled=True)  88.8 us
    reduce_scatter x1, waiting for transfers between devices, per_device(): lax.psum_scatter(terms.reshape(1 * lax.axis_size('tp'), n_sp, local_exper...  83.8 us
    all_to_all x1, blocking collectives, per_device(): lax.all_to_all(results, 'sp', split_axis=0, concat_axis=0, tiled=True)  19.3 us
    all_to_all x1, blocking collectives, per_device(): lax.all_to_all(outgoing, 'sp', split_axis=0, concat_axis=0, tiled=True)  18.3 us
    dot_general x1, matrix products, per_device(): jnp.einsum('sklcf,lfd->kslcd', activated, w_down, preferred_element_type=...  14 us
    convert_element_type x2, local copies, waits for them, and re-layouts, per_device(): terms.reshape(1 * lax.axis_size('tp'), n_sp, local_experts * CAP, width)  13 us
    all_to_all x1, waiting for transfers between devices, per_device(): lax.all_to_all(mixed_rows, 'tp', split_axis=0, concat_axis=1, tiled=True)  8.43 us
    dot_general x1, matrix products, per_device(): jnp.einsum('sklcd,ldf->sklcf', arrived, w_up, preferred_element_type=jnp....  8.36 us
  transfers between devices with their start and end apart: 4, of which 3 were waited for; matrix products, arithmetic and copies ran while one was open for 1% of the time, Pallas kernels for 0%

commit v1 on v0

--- a/solution.py
+++ b/solution.py
@@ -1,6 +1,10 @@
+import functools
+
 import jax
 import jax.numpy as jnp
 from jax import lax
+from jax.experimental import pallas as pl
+from jax.experimental.pallas import tpu as pltpu
 from jax.sharding import PartitionSpec as P
 
 GROUPS = 4
@@ -31,6 +35,340 @@
     gate_clip = jnp.minimum(gate_pre, clamp_limit)
     linear = jnp.clip(upward, -clamp_limit, clamp_limit)
     return gate_clip * jax.nn.sigmoid(glu_alpha * gate_clip) * (linear + 1.0)
+
+
+SLOT = 16
+Y_FIRST = 48
+MESH = pl.DeviceIdType.MESH
+
+
+def coords():
+    return lax.axis_index("grp"), lax.axis_index("sp"), lax.axis_index("tp")
+
+
+def line_barrier(n_tp, others):
+    grp, sp, tp = coords()
+    barrier = pltpu.get_barrier_semaphore()
+    for by in others:
+        target = (grp, (sp + by[0]) % 4, (tp + by[1]) % n_tp)
+        pl.semaphore_signal(barrier, inc=1, device_id=target, device_id_type=MESH)
+    pl.semaphore_wait(barrier, len(others))
+
+
+def gather_kernel(n_tp, cuts, row_ref, meta_ref, all_ref, all_meta, send, recv, msend, mrecv, own):
+    grp, sp, tp = coords()
+    yy, core = sp // 2, sp % 2
+    y_other = (1 - yy) * 2 + core
+    c_other = yy * 2 + (1 - core)
+    others = [(a, b) for a in range(4) for b in range(n_tp) if (a, b) != (0, 0)]
+    own_copy = pltpu.make_async_copy(row_ref, all_ref.at[sp, tp], own.at[0])
+    own_copy.start()
+    own_meta = pltpu.make_async_copy(meta_ref, all_meta.at[sp, tp], own.at[1])
+    own_meta.start()
+    line_barrier(n_tp, others)
+
+    def meta_copy(number, by):
+        return pltpu.make_async_remote_copy(
+            src_ref=meta_ref, dst_ref=all_meta.at[sp, tp],
+            send_sem=msend.at[number], recv_sem=mrecv.at[number],
+            device_id=(grp, (sp + by[0]) % 4, (tp + by[1]) % n_tp), device_id_type=MESH)
+
+    own_copy.wait()
+    own_meta.wait()
+
+    def copy(s, t, part, way):
+        target = [(grp, sp, tp + 1), (grp, sp, tp - 1), (grp, y_other, tp), (grp, c_other, tp)][way]
+        first, count = cuts[part]
+        piece = all_ref.at[s, t, pl.ds(first, count)]
+        return pltpu.make_async_remote_copy(
+            src_ref=piece, dst_ref=piece,
+            send_sem=send.at[s, t, part, way], recv_sem=recv.at[s, t, part],
+            device_id=target, device_id_type=MESH)
+
+    def arrived(s, t, part):
+        copy(s, t, part, 3).wait_recv()
+
+    def guarded(cond, what):
+        pl.when(cond)(what)
+
+    sent = []
+
+    def push(cond, s, t, part, way):
+        if way == 0:
+            cond = jnp.logical_and(cond, tp + 1 < n_tp)
+        if way == 1:
+            cond = jnp.logical_and(cond, tp > 0)
+        guarded(cond, lambda: copy(s, t, part, way).start())
+        sent.append((cond, s, t, part, way))
+
+    yes = tp >= 0
+    push(yes, sp, tp, 0, 2)
+    push(yes, sp, tp, 1, 0)
+    push(yes, sp, tp, 1, 1)
+    push(yes, sp, tp, 1, 2)
+    push(yes, sp, tp, 0, 0)
+    push(yes, sp, tp, 0, 1)
+    push(yes, sp, tp, 0, 3)
+    push(yes, sp, tp, 1, 3)
+    for number, by in enumerate(others):
+        meta_copy(number, by).start()
+    arrived(y_other, tp, 0)
+    push(yes, y_other, tp, 0, 0)
+    push(yes, y_other, tp, 0, 1)
+    push(yes, y_other, tp, 0, 3)
+    for dist in range(1, n_tp):
+        for s, part in ((sp, 1), (sp, 0), (y_other, 0)):
+            for way in (0, 1):
+                t = tp - dist if way == 0 else tp + dist
+                cond = t >= 0 if way == 0 else t < n_tp
+                guarded(cond, functools.partial(arrived, s, t, part))
+                push(cond, s, t, part, way)
+                if part == 1:
+                    push(cond, s, t, part, 2)
+                push(cond, s, t, part, 3)
+        for t, cond in (((tp, yes),) if dist == 1 else ()):
+            arrived(y_other, t, 1)
+            push(yes, y_other, t, 1, 3)
+    for dist in range(1, n_tp):
+        for way in (0, 1):
+            t = tp - dist if way == 0 else tp + dist
+            cond = t >= 0 if way == 0 else t < n_tp
+            guarded(cond, functools.partial(arrived, y_other, t, 1))
+            push(cond, y_other, t, 1, 3)
+    cross = (yes, c_other), (yes, (1 - yy) * 2 + (1 - core))
+    for _, s in cross:
+        for t in range(n_tp):
+            for part in (0, 1):
+                arrived(s, t, part)
+    for cond, s, t, part, way in sent:
+        guarded(cond, lambda s=s, t=t, part=part, way=way: copy(s, t, part, way).wait_send())
+    for number, by in enumerate(others):
+        meta_copy(number, by).wait()
+
+
+def gather_all(normed, meta, n_tp):
+    tok, width = normed.shape
+    first = min(Y_FIRST, tok // 2)
+    cuts = ((0, first), (first, tok - first))
+    vmem = pl.BlockSpec(memory_space=pltpu.VMEM)
+    return pl.pallas_call(
+        functools.partial(gather_kernel, n_tp, cuts),
+        out_shape=(
+            jax.ShapeDtypeStruct((4, n_tp, tok, width), normed.dtype),
+            jax.ShapeDtypeStruct((4, n_tp) + meta.shape, meta.dtype),
+        ),
+        in_specs=[vmem, vmem],
+        out_specs=(vmem, vmem),
+        scratch_shapes=[
+            pltpu.SemaphoreType.DMA((4, n_tp, 2, 4)),
+            pltpu.SemaphoreType.DMA((4, n_tp, 2)),
+            pltpu.SemaphoreType.DMA((4 * n_tp - 1,)),
+            pltpu.SemaphoreType.DMA((4 * n_tp - 1,)),
+            pltpu.SemaphoreType.DMA((2,)),
+        ],
+        compiler_params=pltpu.CompilerParams(
+            collective_id=0, has_side_effects=True, vmem_limit_bytes=40 * 2**20
+        ),
+        name="gather_rows",
+    )(normed, meta)
+
+
+def add_into(dst, src):
+    rows = dst.shape[0]
+    strip = 16
+
+    def body(i, carry):
+        at = pl.ds(pl.multiple_of(i * strip, strip), strip)
+        dst[at] = (dst[at].astype(jnp.float32) + src[at].astype(jnp.float32)).astype(dst.dtype)
+        return carry
+
+    lax.fori_loop(0, rows // strip, body, 0)
+
+
+def scatter_kernel(n_tp, cuts, part_ref, out_ref, work, from_core, za, zb, ya, yb,
+                   csend, crecv, asend, arecv, bsend, brecv, ysend, yrecv, own):
+    grp, sp, tp = coords()
+    yy, core = sp // 2, sp % 2
+    yo = 1 - yy
+    y_other = yo * 2 + core
+    c_other = yy * 2 + (1 - core)
+    nears = [(grp, y_other, tp), (grp, c_other, tp)]
+    barrier = pltpu.get_barrier_semaphore()
+    for target in nears:
+        pl.semaphore_signal(barrier, inc=1, device_id=target, device_id_type=MESH)
+    up_ok, down_ok = tp + 1 < n_tp, tp > 0
+    ups, downs = (grp, sp, tp + 1), (grp, sp, tp - 1)
+    for ok, target in ((up_ok, ups), (down_ok, downs)):
+        pl.when(ok)(lambda target=target: pl.semaphore_signal(
+            barrier, inc=1, device_id=target, device_id_type=MESH))
+    pl.semaphore_wait(barrier, 2 + up_ok.astype(jnp.int32) + down_ok.astype(jnp.int32))
+    (a0, an), (b0, bn) = cuts
+    rows_a, rows_b = pl.ds(a0, an), pl.ds(b0, bn)
+
+    def remote(src, dst, s_sem, r_sem, target):
+        return pltpu.make_async_remote_copy(
+            src_ref=src, dst_ref=dst, send_sem=s_sem, recv_sem=r_sem,
+            device_id=target, device_id_type=MESH)
+
+    def core_copy(y, t):
+        return remote(part_ref.at[y * 2 + (1 - core), t], from_core.at[y, t],
+                      csend.at[y, t], crecv.at[y, t], (grp, c_other, tp))
+
+    order = []
+    for dist in range(n_tp - 1, -1, -1):
+        for side in (1, -1) if dist else (1,):
+            t = tp + side * dist
+            order.append((jnp.logical_and(t >= 0, t < n_tp), t, side, dist))
+    for y in (yo, yy):
+        for ok, t, side, dist in order:
+            pl.when(ok)(lambda y=y, t=t: core_copy(y, t).start())
+    for y in (0, 1):
+        for t in range(n_tp):
+            pltpu.make_async_copy(part_ref.at[y * 2 + core, t], work.at[y, t], own.at[y, t]).start()
+
+    def y_copy_b(t):
+        return remote(work.at[yo, t, rows_b], yb.at[t], ysend.at[t], yrecv.at[t], (grp, y_other, tp))
+
+    def y_copy_a():
+        return remote(work.at[yo, tp, rows_a], ya, ysend.at[n_tp], yrecv.at[n_tp], (grp, y_other, tp))
+
+    def local(y, t):
+        pltpu.make_async_copy(part_ref.at[y * 2 + core, t], work.at[y, t], own.at[y, t]).wait()
+        core_copy(y, t).wait_recv()
+        add_into(work.at[y, t], from_core.at[y, t])
+
+    def z_copy(part, y, t, side):
+        buf, ss, rs, rows = ((za, asend, arecv, rows_a), (zb, bsend, brecv, rows_b))[part]
+        if side == 1:
+            slot, target = t, ups
+        else:
+            slot = jnp.where(t == tp - 1, n_tp, t)
+            target = downs
+        row = y if part == 0 else 0
+        return remote(work.at[y, t, rows], buf.at[row, slot], ss.at[row, t], rs.at[row, slot], target)
+
+    def take_z(part, y, t, slot):
+        buf, ss, rs, rows = ((za, asend, arecv, rows_a), (zb, bsend, brecv, rows_b))[part]
+        row = y if part == 0 else 0
+        remote(work.at[y, t, rows], buf.at[row, slot], ss.at[row, t], rs.at[row, slot], ups).wait_recv()
+        add_into(work.at[y, t, rows], buf.at[row, slot])
+
+    def z_step(part, y, t, side):
+        inner = tp > 0 if side == 1 else tp + 1 < n_tp
+        pl.when(inner)(lambda: take_z(part, y, t, t))
+        z_copy(part, y, t, side).start()
+
+    def z_end(part, y):
+        pl.when(down_ok)(lambda: take_z(part, y, tp, tp))
+        pl.when(up_ok)(lambda: take_z(part, y, tp, n_tp))
+
+    for ok, t, side, dist in order:
+        @pl.when(ok)
+        def _(t=t):
+            local(yo, t)
+            y_copy_b(t).start()
+    for ok, t, side, dist in order:
+        @pl.when(ok)
+        def _(t=t, side=side, dist=dist):
+            local(yy, t)
+            if dist:
+                z_step(0, yo, t, side)
+                z_step(0, yy, t, side)
+            y_copy_b(t).wait_recv()
+            add_into(work.at[yy, t, rows_b], yb.at[t])
+            if dist:
+                z_step(1, yy, t, side)
+    z_end(0, yo)
+    y_copy_a().start()
+    z_end(0, yy)
+    z_end(1, yy)
+    y_copy_a().wait_recv()
+    add_into(work.at[yy, tp, rows_a], ya)
+    last = pltpu.make_async_copy(work.at[yy, tp], out_ref, own.at[0, 0])
+    last.start()
+    last.wait()
+    y_copy_a().wait_send()
+    for ok, t, side, dist in order:
+        @pl.when(ok)
+        def _(t=t, side=side, dist=dist):
+            core_copy(yo, t).wait_send()
+            core_copy(yy, t).wait_send()
+            y_copy_b(t).wait_send()
+            if dist:
+                z_copy(0, yo, t, side).wait_send()
+                z_copy(0, yy, t, side).wait_send()
+                z_copy(1, yy, t, side).wait_send()
+
+
+def scatter_sums(parts, n_tp):
+    tok, width = parts.shape[2:]
+    first = min(Y_FIRST, tok // 2)
+    cuts = ((0, first), (first, tok - first))
+    an, bn = cuts[0][1], cuts[1][1]
+    vmem = pl.BlockSpec(memory_space=pltpu.VMEM)
+    kind = parts.dtype
+    return pl.pallas_call(
+        functools.partial(scatter_kernel, n_tp, cuts),
+        out_shape=jax.ShapeDtypeStruct((tok, width), kind),
+        in_specs=[vmem],
+        out_specs=vmem,
+        scratch_shapes=[
+            pltpu.VMEM((2, n_tp, tok, width), kind),
+            pltpu.VMEM((2, n_tp, tok, width), kind),
+            pltpu.VMEM((2, n_tp + 1, an, width), kind),
+            pltpu.VMEM((1, n_tp + 1, bn, width), kind),
+            pltpu.VMEM((an, width), kind),
+            pltpu.VMEM((n_tp, bn, width), kind),
+            pltpu.SemaphoreType.DMA((2, n_tp)),
+            pltpu.SemaphoreType.DMA((2, n_tp)),
+            pltpu.SemaphoreType.DMA((2, n_tp)),
+            pltpu.SemaphoreType.DMA((2, n_tp + 1)),
+            pltpu.SemaphoreType.DMA((1, n_tp)),
+            pltpu.SemaphoreType.DMA((1, n_tp + 1)),
+            pltpu.SemaphoreType.DMA((n_tp + 1,)),
+            pltpu.SemaphoreType.DMA((n_tp + 1,)),
+            pltpu.SemaphoreType.DMA((2, n_tp)),
+        ],
+        compiler_params=pltpu.CompilerParams(
+            collective_id=1, has_side_effects=True, vmem_limit_bytes=48 * 2**20
+        ),
+        name="scatter_sums",
+    )(parts)
+
+
+def dense_experts(normed, routes, route_weight, w_gate, w_up, w_down):
+    n_sp, n_tp = lax.axis_size("sp"), lax.axis_size("tp")
+    tok, width = normed.shape
+    local_experts = w_gate.shape[0]
+    n_experts = local_experts * n_sp
+    flat_route = routes.reshape(-1)
+    onehot = (flat_route[:, None] == lax.iota(jnp.int32, n_experts)[None, :]).astype(jnp.int32)
+    rank = jnp.sum((jnp.cumsum(onehot, axis=0) - onehot) * onehot, axis=1).reshape(tok, TOP)
+    place = (routes * SLOT + rank).astype(jnp.float32)
+    meta = jnp.concatenate([place, route_weight, jnp.zeros((tok, 8 - 2 * TOP), jnp.float32)], axis=1).T
+    rows, metas = gather_all(normed, meta, n_tp)
+    sources = n_sp * n_tp
+    rows = rows.reshape(sources, tok, width)
+    metas = metas.reshape(sources, 8, tok)
+    slots = local_experts * SLOT
+    index = metas[:, :TOP].astype(jnp.int32) - lax.axis_index("sp") * slots
+    hit = index[:, :, None, :] == lax.iota(jnp.int32, slots)[None, None, :, None]
+    weight = jnp.sum(jnp.where(hit, metas[:, TOP : 2 * TOP, None, :], 0.0), axis=(1, 3))
+    pick = jnp.any(hit, axis=1).astype(jnp.bfloat16)
+    held = jnp.einsum("sct,std->scd", pick, rows, preferred_element_type=jnp.float32)
+    held = held.astype(jnp.bfloat16).reshape(sources, local_experts, SLOT, width)
+    held = held.transpose(1, 0, 2, 3).reshape(local_experts, sources * SLOT, width)
+    gate_pre = jnp.einsum("erd,edf->erf", held, w_gate, preferred_element_type=jnp.float32)
+    upward = jnp.einsum("erd,edf->erf", held, w_up, preferred_element_type=jnp.float32)
+    weight = weight.reshape(sources, local_experts, SLOT).transpose(1, 0, 2)
+    activated = clamped_unit(gate_pre, upward) * weight.reshape(local_experts, sources * SLOT, 1)
+    activated = activated.astype(jnp.bfloat16)
+    terms = jnp.einsum("erf,efd->erd", activated, w_down, preferred_element_type=jnp.float32)
+    terms = terms.astype(jnp.bfloat16).reshape(local_experts, sources, SLOT, width)
+    terms = terms.transpose(1, 0, 2, 3).reshape(sources, slots, width)
+    sums = jnp.einsum("sct,scd->std", pick, terms, preferred_element_type=jnp.float32)
+    sums = sums.astype(jnp.bfloat16).reshape(n_sp, n_tp, tok, width)
+    return scatter_sums(sums, n_tp).astype(jnp.float32)
 
 
 def per_device(
@@ -83,6 +421,9 @@
     residual = (resid_in.astype(jnp.float32) + rms_scale(mix_out, mix_gain)).astype(jnp.bfloat16)
     normed = rms_scale(residual.astype(jnp.float32), ffn_gain).astype(jnp.bfloat16)
     width = normed.shape[1]
+    if n_sp == 4 and n_tp <= 4 and tok_rows % 32 == 0 and tok_rows * width <= 128 * 2048:
+        expert_mix = dense_experts(normed, routes, route_weight, w_gate, w_up, w_down)
+        return (residual.astype(jnp.float32) + rms_scale(expert_mix, post_gain)).astype(jnp.bfloat16)
     local_experts = w_gate.shape[0]
     n_experts = local_experts * n_sp
     slot_total = n_experts * CAP

time: 290 us -> 208 us (0.72)
  waiting for transfers between devices: 181 us -> 8.73 us
  Pallas kernels: 0 us -> 117 us
  blocking collectives: 37.6 us -> 0 us
  matrix products: 27 us -> 43.8 us
  between operations: 13.6 us -> 0.25 us
  local copies, waits for them, and re-layouts: 17.3 us -> 23.1 us
    pallas_call x0 -> x2, Pallas kernels: none -> 117 us  [the longest x1 61 us: scatter_sums(): pl.pallas_call(functools.partial(scatter_kernel, n_tp, cuts), out_shape=j...]
    all_gather x1 -> x0, waiting for transfers between devices: 88.8 us -> none  [per_device(): arrived = lax.all_gather(at_owner[:, None], 'tp', axis=1, tiled=True)]
    reduce_scatter x1 -> x0, waiting for transfers between devices: 83.8 us -> none  [per_device(): lax.psum_scatter(terms.reshape(1 * lax.axis_size('tp'), n_sp, local_exper...]
    all_to_all x2 -> x0, blocking collectives: 37.6 us -> none  [the longest x1 19.3 us: per_device(): lax.all_to_all(results, 'sp', split_axis=0, concat_axis=0, tiled=True)]
    dot_general x4 -> x5, matrix products: 23.7 us -> 40.5 us  [the longest x1 9.6 us: dense_experts(): jnp.einsum('erd,edf->erf', held, w_gate, preferred_element_type=jnp.float32)]
    transpose x0 -> x3, local copies, waits for them, and re-layouts: none -> 16.5 us  [the longest x1 8.26 us: dense_experts(): terms = terms.transpose(1, 0, 2, 3).reshape(sources, slots, width)]
    convert_element_type x2 -> x0, local copies, waits for them, and re-layouts: 13 us -> none  [per_device(): terms.reshape(1 * lax.axis_size('tp'), n_sp, local_experts * CAP, width)]
    unnamed x17 -> x25, local copies, waits for them, and re-layouts: 0.83 us -> 4.03 us
  transfers between devices with their start and end apart: 4 -> 2, of which waited for: 3 -> 1; matrix products, arithmetic and copies ran while one was open for 1% -> 1% of each run, Pallas kernels for 0% -> 0%
where the time goes in v1:
time: 208 us; the launch traced here: 207 us
  Pallas kernels  117 us (56%)
  matrix products  43.8 us (21%)
  local copies, waits for them, and re-layouts  23.1 us (11%)
  waiting for transfers between devices  8.73 us (4%)
  starting transfers between devices  8.08 us (4%)
  other arithmetic  6.21 us (3%)
    pallas_call x1, Pallas kernels, scatter_sums(): pl.pallas_call(functools.partial(scatter_kernel, n_tp, cuts), out_shape=j...  61 us
    pallas_call x1, Pallas kernels, gather_all(): pl.pallas_call(functools.partial(gather_kernel, n_tp, cuts), out_shape=(j...  56.1 us
    dot_general x1, matrix products, dense_experts(): jnp.einsum('erd,edf->erf', held, w_gate, preferred_element_type=jnp.float32)  9.6 us
    dot_general x1, matrix products, dense_experts(): jnp.einsum('sct,scd->std', pick, terms, preferred_element_type=jnp.float32)  9.03 us
    dot_general x1, matrix products, dense_experts(): jnp.einsum('sct,std->scd', pick, rows, preferred_element_type=jnp.float32)  8.93 us
    all_to_all x1, waiting for transfers between devices, per_device(): lax.all_to_all(mixed_rows, 'tp', split_axis=0, concat_axis=1, tiled=True)  8.73 us
    transpose x1, local copies, waits for them, and re-layouts, dense_experts(): terms = terms.transpose(1, 0, 2, 3).reshape(sources, slots, width)  8.26 us
    transpose x1, local copies, waits for them, and re-layouts, dense_experts(): held.transpose(1, 0, 2, 3).reshape(local_experts, sources * SLOT, width)  8.25 us
  transfers between devices with their start and end apart: 2, of which 1 were waited for; matrix products, arithmetic and copies ran while one was open for 1% of the time, Pallas kernels for 0%

profile of v1, /device:TPU:0, one launch (start us, length us, event | category | flops | bytes accessed | tf_op | source)
XLA Modules:
  0.0 207.3 jit_solution(9233188141234261012)
XLA Ops:
  0.0 0.0 copy-start
  0.0 0.0 copy-start.8
  0.0 0.0 copy-start.9
  0.0 0.8 slice.64
  0.8 2.4 %collective-permute-start = (bf16[15,256]{1,0:T(8,128)(2,1)S(1)}, bf16[15,256]{1,0:T(8,128)(2,1)S(1)}, u32[]{:S(2)}, u32[]{:S(2)}) collective-permute-start(bf16[15,256]{1,0:T(8,128)(2,1)S(1)} %slice.64), channel_id=1, source_target_pairs={{0,4},{4,8},{8,12},{1,5},{5,9},{9,13},{2,6},{6,10},{10,14},{3,7},{... | collective-permute-start | bytes 23048 | tf_op jit(solution)/shard_map/ppermute | solution.py:26
  3.2 0.8 copy.35
  4.0 0.1 eq.171
  4.1 0.1 eq.167
  4.3 0.6 reduce-window.6
  4.9 0.2 slice_reduce_fusion
  5.1 0.1 fusion.16
  5.3 0.7 mul.110
  6.0 0.1 reshape.135
  6.1 0.1 copy.38
  6.2 0.1 pad.2.clone
  6.2 0.0 copy-start.4
  6.2 0.0 copy-start.5
  6.3 0.0 collective-permute-done
  6.3 1.1 maximum_convert_fusion
  7.3 0.0 copy-start.6
  7.3 1.5 fusion.12
  8.8 5.7 %all-to-all-start = ((bf16[4,128,256]{2,1,0:T(8,128)(2,1)}), bf16[4,128,256]{2,1,0:T(8,128)(2,1)S(1)}, u32[]{:S(2)}, u32[]{:S(2)}) async-start(bf16[4,128,256]{2,1,0:T(8,128)(2,1)} %bitcast), calls=%async_computation | async-start | bytes 524288 | tf_op jit(solution)/shard_map/all_to_all | solution.py:409
  14.5 0.0 copy-done.8
  14.5 0.0 copy-done.9
  14.5 0.1 maximum_bitcast_fusion.meta_ref
  14.6 8.7 %all-to-all-done = bf16[4,128,256]{2,1,0:T(8,128)(2,1)S(1)} async-done(((bf16[4,128,256]{2,1,0:T(8,128)(2,1)}), bf16[4,128,256]{2,1,0:T(8,128)(2,1)S(1)}, u32[]{:S(2)}, u32[]{:S(2)}) %all-to-all-start) | async-done | bytes 262176 | tf_op jit(solution)/shard_map/all_to_all | solution.py:409
  23.3 0.0 copy-done
  23.3 0.2 fusion.2
  23.6 0.2 copy.34
  23.8 3.0 %multiply_reduce_fusion = (f32[128]{0:T(128)S(1)}, f32[128,2048]{1,0:T(8,128)S(1)}) fusion(bf16[128,1024]{0,1:T(8,128)(2,1)S(1)} %bitcast.64, bf16[1024,2048]{1,0:T(8,128)(2,1)} %param.17), kind=kOutput, calls=%fused_computation.22 | convolution fusion | flops 537395072 | bytes 5505536 | tf_op jit(solution)/shard_map/dot_general | solution.py:420
  26.8 0.0 copy-done.4
  26.8 0.0 copy-done.5
  26.8 0.4 fusion.5
  27.2 0.0 copy-done.6
  27.2 0.2 fusion.7.row_ref
  27.4 56.1 %gather_rows.1 = (bf16[4,4,128,2048]{3,2,1,0:T(8,128)(2,1)S(1)}, f32[4,4,8,128]{3,2,1,0:T(8,128)S(1)}) custom-call(bf16[128,2048]{1,0:T(8,128)(2,1)S(1)} %fusion.7.row_ref, f32[8,128]{1,0:T(8,128)S(1)} %maximum_bitcast_fusion.meta_ref), custom_call_target="tpu_custom_call" | custom-call | tf_op jit(solution)/shard_map/gather_rows/pallas_call | solution.py:154
  83.5 0.0 copy-start.2
  83.6 3.2 %copy-done.2 = bf16[4,4,128,2048]{3,2,1,0:T(8,128)(2,1)} copy-done((bf16[4,4,128,2048]{3,2,1,0:T(8,128)(2,1)}, bf16[4,4,128,2048]{3,2,1,0:T(8,128)(2,1)S(1)}, u32[]{:S(2)}) %copy-start.2) | copy-done | bytes 8388632
  86.8 0.5 fusion
  87.3 0.4 select_reduce_fusion
  87.7 0.1 reshape.140
  87.8 0.1 mul.131
  87.9 8.9 %convolution_convert_fusion.2 = bf16[16,128,2048]{2,1,0:T(8,128)(2,1)} fusion(pred[16,128,128]{2,1,0:T(8,128)(4,1)S(1)} %fusion, bf16[16,128,2048]{2,1,0:T(8,128)(2,1)} %bitcast.53), kind=kOutput, calls=%fused_computation.2 | convolution fusion | flops 1077936128 | bytes 17039360 | tf_op jit(solution)/shard_map/sct,std->scd/dot_general | solution.py:358
  96.9 8.3 %copy.39 = bf16[8,16,16,2048]{3,2,1,0:T(8,128)(2,1)} copy(bf16[8,16,16,2048]{3,2,0,1:T(8,128)(2,1)} %bitcast.58) | data formatting | bytes 16777216 | tf_op jit(solution)/shard_map/transpose | solution.py:360
  105.1 0.0 copy-start.3
  105.1 0.0 slice-start
  105.1 9.6 %fusion.19 = f32[8,256,256]{2,1,0:T(8,128)} fusion(bf16[8,256,2048]{2,1,0:T(8,128)(2,1)} %bitcast.62, bf16[8,2048,256]{2,1,0:T(8,128)(2,1)} %param.20), kind=kOutput, calls=%fused_computation.73 | convolution fusion | flops 2147483648 | bytes 18874368 | tf_op jit(solution)/shard_map/erd,edf->erf/dot_general | solution.py:361
  114.7 0.0 copy-done.3
  114.7 0.0 slice-start.1
  114.7 7.2 %multiply_convert_fusion = bf16[8,256,256]{2,1,0:T(8,128)(2,1)S(1)} fusion(f32[8,256,256]{2,1,0:T(8,128)} %fusion.19, bf16[8,256,2048]{2,1,0:T(8,128)(2,1)S(1)} %bitcast.63, bf16[8,2048,256]{2,1,0:T(8,128)(2,1)} %param.21, f32[8,256]{1,0:T(8,128)S(1)} %mul.131), kind=kOutput, calls=%fused_computation.3 | convolution fusion | flops 2153250816 | bytes 19931136 | tf_op jit(solution)/shard_map/erd,edf->erf/dot_general | solution.py:362
  121.9 0.0 slice-done
  121.9 0.0 slice-done.1
  121.9 5.8 %convolution_convert_fusion.1 = bf16[8,256,2048]{2,1,0:T(8,128)(2,1)} fusion(bf16[8,256,256]{2,1,0:T(8,128)(2,1)S(1)} %multiply_convert_fusion, bf16[8,256,2048]{2,1,0:T(8,128)(2,1)S(1)} %bitcast.61), kind=kOutput, calls=%fused_computation.1 | convolution fusion | flops 2151677952 | bytes 17825792 | tf_op jit(solution)/shard_map/erf,efd->erd/dot_general | solution.py:366
  127.7 8.3 %copy.41 = bf16[16,8,16,2048]{3,2,1,0:T(8,128)(2,1)} copy(bf16[16,8,16,2048]{3,2,0,1:T(8,128)(2,1)} %bitcast.59) | data formatting | bytes 16777216 | tf_op jit(solution)/shard_map/transpose | solution.py:368
  136.0 0.0 copy-start.1
  136.0 9.0 %convolution_convert_fusion = bf16[16,128,2048]{2,1,0:T(8,128)(2,1)} fusion(pred[16,128,128]{2,1,0:T(8,128)(4,1)S(1)} %fusion, bf16[16,128,2048]{2,1,0:T(8,128)(2,1)} %bitcast.56), kind=kOutput, calls=%fused_computation | convolution fusion | flops 1077936128 | bytes 17039360 | tf_op jit(solution)/shard_map/sct,scd->std/dot_general | solution.py:369
  145.0 0.0 copy-start.7
  145.0 61.0 %scatter_sums.1 = bf16[128,2048]{1,0:T(8,128)(2,1)S(1)} custom-call(bf16[4,4,128,2048]{3,2,1,0:T(8,128)(2,1)} %bitcast.57), custom_call_target="tpu_custom_call" | custom-call | tf_op jit(solution)/shard_map/scatter_sums/pallas_call | solution.py:310
  206.0 0.2 fusion.3
  206.2 0.0 copy-done.7
  206.2 1.1 fusion.8
  207.3 0.0 copy-done.1
  (16 shorter events, 0.2 us)
Async XLA Ops:
  0.0 23.3 %copy-start = (bf16[4,256,256]{2,1,0:T(8,128)(2,1)S(1)}, bf16[4,256,256]{2,1,0:T(8,128)(2,1)}, u32[]{:S(2)}) copy-start(bf16[4,256,256]{2,1,0:T(8,128)(2,1)} %param.15) | copy-start | bytes 1572868
  0.0 14.5 %copy-start.8 = (s32[128,2]{0,1:T(2,128)S(1)}, s32[128,2]{0,1:T(2,128)}, u32[]{:S(2)}) copy-start(s32[128,2]{0,1:T(2,128)} %param.23) | copy-start | bytes 3076
  0.0 14.5 %copy-start.9 = (f32[128,2]{0,1:T(2,128)S(1)}, f32[128,2]{0,1:T(2,128)}, u32[]{:S(2)}) copy-start(f32[128,2]{0,1:T(2,128)} %param.24) | copy-start | bytes 3076
  0.8 5.5 %collective-permute-start = (bf16[15,256]{1,0:T(8,128)(2,1)S(1)}, bf16[15,256]{1,0:T(8,128)(2,1)S(1)}, u32[]{:S(2)}, u32[]{:S(2)}) collective-permute-start(bf16[15,256]{1,0:T(8,128)(2,1)S(1)} %slice.64), channel_id=1, source_target_pairs={{0,4},{4,8},{8,12},{1,5},{5,9},{9,13},{2,6},{6,10},{10,14},{3,7},{... | collective-permute-start | bytes 23048 | tf_op jit(solution)/shard_map/ppermute | solution.py:26
  6.2 20.5 %copy-start.4 = (bf16[128,2048]{1,0:T(8,128)(2,1)S(1)}, bf16[128,2048]{1,0:T(8,128)(2,1)}, u32[]{:S(2)}) copy-start(bf16[128,2048]{1,0:T(8,128)(2,1)} %param.13) | copy-start | bytes 1572868
  6.2 20.6 %copy-start.5 = (f32[2048]{0:T(1024)S(1)}, f32[2048]{0:T(1024)}, u32[]{:S(2)}) copy-start(f32[2048]{0:T(1024)} %param.18) | copy-start | bytes 24580
  7.3 19.9 %copy-start.6 = (f32[2048]{0:T(1024)S(1)}, f32[2048]{0:T(1024)}, u32[]{:S(2)}) copy-start(f32[2048]{0:T(1024)} %param.19) | copy-start | bytes 24580
  8.8 14.5 %all-to-all-start = ((bf16[4,128,256]{2,1,0:T(8,128)(2,1)}), bf16[4,128,256]{2,1,0:T(8,128)(2,1)S(1)}, u32[]{:S(2)}, u32[]{:S(2)}) async-start(bf16[4,128,256]{2,1,0:T(8,128)(2,1)} %bitcast), calls=%async_computation | async-start | bytes 524288 | tf_op jit(solution)/shard_map/all_to_all | solution.py:409
  83.5 3.2 %copy-start.2 = (bf16[4,4,128,2048]{3,2,1,0:T(8,128)(2,1)}, bf16[4,4,128,2048]{3,2,1,0:T(8,128)(2,1)S(1)}, u32[]{:S(2)}) copy-start(bf16[4,4,128,2048]{3,2,1,0:T(8,128)(2,1)S(1)} %get-tuple-element.8) | copy-start | bytes 25165828
  105.1 9.6 %copy-start.3 = (bf16[8,16,16,2048]{3,2,1,0:T(8,128)(2,1)S(1)}, bf16[8,16,16,2048]{3,2,1,0:T(8,128)(2,1)}, u32[]{:S(2)}) copy-start(bf16[8,16,16,2048]{3,2,1,0:T(8,128)(2,1)} %copy.39) | copy-start | bytes 25165828
  105.1 16.8 %slice-start = ((s8[8388608]{0:T(1024)(128)(4,1)}), s8[4194304]{0:T(1024)(128)(4,1)S(1)}, s32[]{:S(2)}) async-start(s8[8388608]{0:T(1024)(128)(4,1)} %bitcast.60), calls=%async_computation.1 | async-start | bytes 8388608
  114.7 7.2 %slice-start.1 = ((s8[8388608]{0:T(1024)(128)(4,1)}), s8[4194304]{0:T(1024)(128)(4,1)S(1)}, s32[]{:S(2)}) async-start(s8[8388608]{0:T(1024)(128)(4,1)} %bitcast.60), calls=%async_computation.2 | async-start | bytes 8388608
  136.0 71.3 %copy-start.1 = (bf16[4,256,256]{2,1,0:T(8,128)(2,1)S(1)}, bf16[4,256,256]{2,1,0:T(8,128)(2,1)}, u32[]{:S(2)}) copy-start(bf16[4,256,256]{2,1,0:T(8,128)(2,1)} %param.15) | copy-start | bytes 1572868
  145.0 61.2 %copy-start.7 = (f32[2048]{0:T(1024)S(1)}, f32[2048]{0:T(1024)}, u32[]{:S(2)}) copy-start(f32[2048]{0:T(1024)} %param.25) | copy-start | bytes 24580

commit v2 on v0

--- a/solution.py
+++ b/solution.py
@@ -1,6 +1,10 @@
+import functools
+
 import jax
 import jax.numpy as jnp
 from jax import lax
+from jax.experimental import pallas as pl
+from jax.experimental.pallas import tpu as pltpu
 from jax.sharding import PartitionSpec as P
 
 GROUPS = 4
@@ -31,6 +35,381 @@
     gate_clip = jnp.minimum(gate_pre, clamp_limit)
     linear = jnp.clip(upward, -clamp_limit, clamp_limit)
     return gate_clip * jax.nn.sigmoid(glu_alpha * gate_clip) * (linear + 1.0)
+
+
+SLOT = 16
+Y_FIRST = 16
+MESH = pl.DeviceIdType.MESH
+
+
+def coords():
+    return lax.axis_index("grp"), lax.axis_index("sp"), lax.axis_index("tp")
+
+
+def layer_kernel(n_tp, cuts, row_ref, meta_ref, wg_ref, wu_ref, wd_ref, out_ref,
+                 every, metas, picks, weights, held, wg, wu, wd,
+                 work, from_core, za, zb, ya, yb,
+                 send, recv, msend, mrecv, wsem,
+                 csend, crecv, asend, arecv, bsend, brecv, ysend, yrecv, own):
+    grp, sp, tp = coords()
+    yy, core = sp // 2, sp % 2
+    yo = 1 - yy
+    y_other = yo * 2 + core
+    c_other = yy * 2 + (1 - core)
+    tok, width = row_ref.shape
+    local_experts, buffers = wg_ref.shape[0], wg.shape[0]
+    slots = local_experts * SLOT
+    chunk = min(512, width)
+    others = [(a, b) for a in range(4) for b in range(n_tp) if (a, b) != (0, 0)]
+
+    def weight_copies(e):
+        at = lax.rem(e, buffers)
+        return [pltpu.make_async_copy(w.at[e], buf.at[at], wsem.at[i, at])
+                for i, (w, buf) in enumerate(((wg_ref, wg), (wu_ref, wu), (wd_ref, wd)))]
+
+    own_copy = pltpu.make_async_copy(row_ref, every.at[sp, tp], own.at[0, 0])
+    own_copy.start()
+    own_meta = pltpu.make_async_copy(meta_ref, metas.at[sp, tp], own.at[0, 1])
+    own_meta.start()
+    barrier = pltpu.get_barrier_semaphore()
+    for by in others:
+        target = (grp, (sp + by[0]) % 4, (tp + by[1]) % n_tp)
+        pl.semaphore_signal(barrier, inc=1, device_id=target, device_id_type=MESH)
+    pl.semaphore_wait(barrier, len(others))
+
+    def meta_copy(number, by):
+        return pltpu.make_async_remote_copy(
+            src_ref=meta_ref, dst_ref=metas.at[sp, tp],
+            send_sem=msend.at[number], recv_sem=mrecv.at[number],
+            device_id=(grp, (sp + by[0]) % 4, (tp + by[1]) % n_tp), device_id_type=MESH)
+
+    own_copy.wait()
+    own_meta.wait()
+
+    def copy(s, t, part, way):
+        target = [(grp, sp, tp + 1), (grp, sp, tp - 1), (grp, y_other, tp), (grp, c_other, tp)][way]
+        first, count = cuts[part]
+        piece = every.at[s, t, pl.ds(first, count)]
+        return pltpu.make_async_remote_copy(
+            src_ref=piece, dst_ref=piece,
+            send_sem=send.at[s, t, part, way], recv_sem=recv.at[s, t, part],
+            device_id=target, device_id_type=MESH)
+
+    def arrived(s, t, part):
+        copy(s, t, part, 3).wait_recv()
+
+    sent = []
+
+    def push(cond, s, t, part, way):
+        if way == 0:
+            cond = jnp.logical_and(cond, tp + 1 < n_tp)
+        if way == 1:
+            cond = jnp.logical_and(cond, tp > 0)
+        pl.when(cond)(lambda: copy(s, t, part, way).start())
+        sent.append((cond, s, t, part, way))
+
+    def source_rows(s, t):
+        return pl.ds(pl.multiple_of((s * n_tp + t) * SLOT, SLOT), SLOT)
+
+    def select(s, t):
+        slot = lax.broadcasted_iota(jnp.int32, (slots, tok), 0).astype(jnp.float32)
+        base = (sp * slots).astype(jnp.float32)
+        meta = metas[s, t]
+        pick = jnp.zeros((slots, tok), jnp.float32)
+        weight = jnp.zeros((slots, tok), jnp.float32)
+        for k in range(TOP):
+            hit = (meta[k : k + 1] - base) == slot
+            pick = pick + jnp.where(hit, 1.0, 0.0)
+            weight = weight + jnp.where(hit, meta[TOP + k : TOP + k + 1], 0.0)
+        weight = jnp.broadcast_to(jnp.sum(weight, axis=1, keepdims=True), (slots, 128))
+        pick = pick.astype(jnp.bfloat16)
+        picks[s, t] = pick
+        for e in range(local_experts):
+            weights[e, source_rows(s, t)] = weight[e * SLOT : (e + 1) * SLOT]
+
+        def body(i, carry):
+            at = pl.ds(pl.multiple_of(i * chunk, chunk), chunk)
+            got = jnp.dot(pick, every[s, t, :, at], preferred_element_type=jnp.float32)
+            got = got.astype(jnp.bfloat16)
+            for e in range(local_experts):
+                held[e, source_rows(s, t), at] = got[e * SLOT : (e + 1) * SLOT]
+            return carry
+
+        lax.fori_loop(0, width // chunk, body, 0)
+
+    yes = tp >= 0
+    for number, by in enumerate(others):
+        meta_copy(number, by).start()
+    push(yes, sp, tp, 0, 2)
+    push(yes, sp, tp, 1, 0)
+    push(yes, sp, tp, 1, 1)
+    push(yes, sp, tp, 1, 2)
+    push(yes, sp, tp, 0, 0)
+    push(yes, sp, tp, 0, 1)
+    push(yes, sp, tp, 0, 3)
+    push(yes, sp, tp, 1, 3)
+    for e in range(min(buffers, local_experts)):
+        for c in weight_copies(e):
+            c.start()
+    arrived(y_other, tp, 0)
+    push(yes, y_other, tp, 0, 0)
+    push(yes, y_other, tp, 0, 1)
+    push(yes, y_other, tp, 0, 3)
+    select(sp, tp)
+    for number, by in enumerate(others):
+        meta_copy(number, by).wait()
+    for dist in range(1, n_tp):
+        for s, part in ((sp, 1), (sp, 0), (y_other, 0)):
+            for way in (0, 1):
+                t = tp - dist if way == 0 else tp + dist
+                cond = t >= 0 if way == 0 else t < n_tp
+                pl.when(cond)(functools.partial(arrived, s, t, part))
+                push(cond, s, t, part, way)
+                if part == 1:
+                    push(cond, s, t, part, 2)
+                push(cond, s, t, part, 3)
+        if dist == 1:
+            arrived(y_other, tp, 1)
+            push(yes, y_other, tp, 1, 3)
+            select(y_other, tp)
+        for way in (0, 1):
+            t = tp - dist if way == 0 else tp + dist
+            cond = t >= 0 if way == 0 else t < n_tp
+            pl.when(cond)(functools.partial(select, sp, t))
+    for dist in range(1, n_tp):
+        for way in (0, 1):
+            t = tp - dist if way == 0 else tp + dist
+            cond = t >= 0 if way == 0 else t < n_tp
+            pl.when(cond)(functools.partial(arrived, y_other, t, 1))
+            push(cond, y_other, t, 1, 3)
+            pl.when(cond)(functools.partial(select, y_other, t))
+    for s in (c_other, yo * 2 + (1 - core)):
+        def cross(t, carry, s=s):
+            for part in (0, 1):
+                arrived(s, t, part)
+            select(s, t)
+            return carry
+
+        lax.fori_loop(0, n_tp, cross, 0)
+    for cond, s, t, part, way in sent:
+        pl.when(cond)(lambda s=s, t=t, part=part, way=way: copy(s, t, part, way).wait_send())
+
+    def expert(e, carry):
+        at = lax.rem(e, buffers)
+        for c in weight_copies(e):
+            c.wait()
+        rows = held[e]
+        gate_pre = jnp.dot(rows, wg[at], preferred_element_type=jnp.float32)
+        upward = jnp.dot(rows, wu[at], preferred_element_type=jnp.float32)
+        scale = jnp.concatenate([weights[e]] * (gate_pre.shape[1] // 128), axis=1)
+        activated = (clamped_unit(gate_pre, upward) * scale).astype(jnp.bfloat16)
+
+        def down(i, inner):
+            cols = pl.ds(pl.multiple_of(i * chunk, chunk), chunk)
+            term = jnp.dot(activated, wd[at, :, cols], preferred_element_type=jnp.float32)
+            held[e, :, cols] = term.astype(jnp.bfloat16)
+            return inner
+
+        lax.fori_loop(0, width // chunk, down, 0)
+
+        @pl.when(e + buffers < local_experts)
+        def _():
+            for c in weight_copies(e + buffers):
+                c.start()
+
+        return carry
+
+    lax.fori_loop(0, local_experts, expert, 0)
+
+    def combined(s, t, at):
+        term = held[:, source_rows(s, t), at].reshape(slots, chunk)
+        return lax.dot_general(picks[s, t], term, (((0,), (0,)), ((), ())),
+                               preferred_element_type=jnp.float32)
+
+    (a0, an), (b0, bn) = cuts
+    rows_a, rows_b = pl.ds(a0, an), pl.ds(b0, bn)
+    ups, downs = (grp, sp, tp + 1), (grp, sp, tp - 1)
+    up_ok, down_ok = tp + 1 < n_tp, tp > 0
+
+    def remote(src, dst, s_sem, r_sem, target):
+        return pltpu.make_async_remote_copy(
+            src_ref=src, dst_ref=dst, send_sem=s_sem, recv_sem=r_sem,
+            device_id=target, device_id_type=MESH)
+
+    def core_copy(y, t):
+        return remote(every.at[y * 2 + (1 - core), t], from_core.at[y, t],
+                      csend.at[y, t], crecv.at[y, t], (grp, c_other, tp))
+
+    def combine_away(y, t):
+        s = y * 2 + (1 - core)
+
+        def body(i, carry):
+            at = pl.ds(pl.multiple_of(i * chunk, chunk), chunk)
+            every[s, t, :, at] = combined(s, t, at).astype(jnp.bfloat16)
+            return carry
+
+        lax.fori_loop(0, width // chunk, body, 0)
+        core_copy(y, t).start()
+
+    order = []
+    for dist in range(n_tp - 1, -1, -1):
+        for side in (1, -1) if dist else (1,):
+            t = tp + side * dist
+            order.append((jnp.logical_and(t >= 0, t < n_tp), t, side, dist))
+
+    def y_copy_b(t):
+        return remote(work.at[yo, t, rows_b], yb.at[t], ysend.at[t], yrecv.at[t], (grp, y_other, tp))
+
+    def y_copy_a():
+        return remote(work.at[yo, tp, rows_a], ya, ysend.at[n_tp], yrecv.at[n_tp], (grp, y_other, tp))
+
+    def local(y, t):
+        s = y * 2 + core
+        core_copy(y, t).wait_recv()
+
+        def body(i, carry):
+            at = pl.ds(pl.multiple_of(i * chunk, chunk), chunk)
+            both = combined(s, t, at) + from_core[y, t, :, at].astype(jnp.float32)
+            work[y, t, :, at] = both.astype(jnp.bfloat16)
+            return carry
+
+        lax.fori_loop(0, width // chunk, body, 0)
+
+    def z_copy(part, y, t, side):
+        buf, ss, rs, rows = ((za, asend, arecv, rows_a), (zb, bsend, brecv, rows_b))[part]
+        if side == 1:
+            slot, target = t, ups
+        else:
+            slot = jnp.where(t == tp - 1, n_tp, t)
+            target = downs
+        row = y if part == 0 else 0
+        return remote(work.at[y, t, rows], buf.at[row, slot], ss.at[row, t], rs.at[row, slot], target)
+
+    def take_z(part, y, t, slot):
+        buf, ss, rs, rows = ((za, asend, arecv, rows_a), (zb, bsend, brecv, rows_b))[part]
+        row = y if part == 0 else 0
+        remote(work.at[y, t, rows], buf.at[row, slot], ss.at[row, t], rs.at[row, slot], ups).wait_recv()
+        add_into(work.at[y, t, rows], buf.at[row, slot])
+
+    def z_step(part, y, t, side):
+        inner = tp > 0 if side == 1 else tp + 1 < n_tp
+        pl.when(inner)(lambda: take_z(part, y, t, t))
+        z_copy(part, y, t, side).start()
+
+    def z_end(part, y):
+        pl.when(down_ok)(lambda: take_z(part, y, tp, tp))
+        pl.when(up_ok)(lambda: take_z(part, y, tp, n_tp))
+
+    for y in (yo, yy):
+        for ok, t, side, dist in order:
+            pl.when(ok)(functools.partial(combine_away, y, t))
+        if y is yo:
+            for ok, t, side, dist in order:
+                @pl.when(ok)
+                def _(t=t):
+                    local(yo, t)
+                    y_copy_b(t).start()
+    for ok, t, side, dist in order:
+        @pl.when(ok)
+        def _(t=t, side=side, dist=dist):
+            local(yy, t)
+            y_copy_b(t).wait_recv()
+            add_into(work.at[yy, t, rows_b], yb.at[t])
+            if dist:
+                z_step(1, yy, t, side)
+                z_step(0, yo, t, side)
+                z_step(0, yy, t, side)
+    z_end(0, yo)
+    y_copy_a().start()
+    z_end(0, yy)
+    z_end(1, yy)
+    y_copy_a().wait_recv()
+    add_into(work.at[yy, tp, rows_a], ya)
+    last = pltpu.make_async_copy(work.at[yy, tp], out_ref, own.at[0, 0])
+    last.start()
+    last.wait()
+    y_copy_a().wait_send()
+    for ok, t, side, dist in order:
+        @pl.when(ok)
+        def _(t=t, side=side, dist=dist):
+            core_copy(yo, t).wait_send()
+            core_copy(yy, t).wait_send()
+            y_copy_b(t).wait_send()
+            if dist:
+                z_copy(0, yo, t, side).wait_send()
+                z_copy(0, yy, t, side).wait_send()
+                z_copy(1, yy, t, side).wait_send()
+
+
+def add_into(dst, src):
+    rows = dst.shape[0]
+    strip = 16
+
+    def body(i, carry):
+        at = pl.ds(pl.multiple_of(i * strip, strip), strip)
+        dst[at] = (dst[at].astype(jnp.float32) + src[at].astype(jnp.float32)).astype(dst.dtype)
+        return carry
+
+    lax.fori_loop(0, rows // strip, body, 0)
+
+
+def dense_experts(normed, routes, route_weight, w_gate, w_up, w_down):
+    n_sp, n_tp = lax.axis_size("sp"), lax.axis_size("tp")
+    tok, width = normed.shape
+    local_experts, _, hidden = w_gate.shape
+    n_experts = local_experts * n_sp
+    flat_route = routes.reshape(-1)
+    onehot = (flat_route[:, None] == lax.iota(jnp.int32, n_experts)[None, :]).astype(jnp.int32)
+    rank = jnp.sum((jnp.cumsum(onehot, axis=0) - onehot) * onehot, axis=1).reshape(tok, TOP)
+    place = (routes * SLOT + rank).astype(jnp.float32)
+    meta = jnp.concatenate([place, route_weight, jnp.zeros((tok, 8 - 2 * TOP), jnp.float32)], axis=1).T
+    cuts = ((0, Y_FIRST), (Y_FIRST, tok - Y_FIRST))
+    an, bn = cuts[0][1], cuts[1][1]
+    vmem, hbm = pl.BlockSpec(memory_space=pltpu.VMEM), pl.BlockSpec(memory_space=pl.ANY)
+    kind = normed.dtype
+    slots, buffers = local_experts * SLOT, min(4, local_experts)
+    dma = pltpu.SemaphoreType.DMA
+    mixed = pl.pallas_call(
+        functools.partial(layer_kernel, n_tp, cuts),
+        out_shape=jax.ShapeDtypeStruct((tok, width), kind),
+        in_specs=[vmem, vmem, hbm, hbm, hbm],
+        out_specs=vmem,
+        scratch_shapes=[
+            pltpu.VMEM((4, n_tp, tok, width), kind),
+            pltpu.VMEM((4, n_tp) + meta.shape, jnp.float32),
+            pltpu.VMEM((4, n_tp, slots, tok), kind),
+            pltpu.VMEM((local_experts, 4 * n_tp * SLOT, 128), jnp.float32),
+            pltpu.VMEM((local_experts, 4 * n_tp * SLOT, width), kind),
+            pltpu.VMEM((buffers, width, hidden), kind),
+            pltpu.VMEM((buffers, width, hidden), kind),
+            pltpu.VMEM((buffers, hidden, width), kind),
+            pltpu.VMEM((2, n_tp, tok, width), kind),
+            pltpu.VMEM((2, n_tp, tok, width), kind),
+            pltpu.VMEM((2, n_tp + 1, an, width), kind),
+            pltpu.VMEM((1, n_tp + 1, bn, width), kind),
+            pltpu.VMEM((an, width), kind),
+            pltpu.VMEM((n_tp, bn, width), kind),
+            dma((4, n_tp, 2, 4)),
+            dma((4, n_tp, 2)),
+            dma((4 * n_tp - 1,)),
+            dma((4 * n_tp - 1,)),
+            dma((3, buffers)),
+            dma((2, n_tp)),
+            dma((2, n_tp)),
+            dma((2, n_tp)),
+            dma((2, n_tp + 1)),
+            dma((1, n_tp)),
+            dma((1, n_tp + 1)),
+            dma((n_tp + 1,)),
+            dma((n_tp + 1,)),
+            dma((2, max(2, n_tp))),
+        ],
+        compiler_params=pltpu.CompilerParams(
+            collective_id=0, has_side_effects=True, vmem_limit_bytes=56 * 2**20
+        ),
+        name="routed_experts",
+    )(normed, meta, w_gate, w_up, w_down)
+    return mixed.astype(jnp.float32)
 
 
 def per_device(
@@ -83,6 +462,9 @@
     residual = (resid_in.astype(jnp.float32) + rms_scale(mix_out, mix_gain)).astype(jnp.bfloat16)
     normed = rms_scale(residual.astype(jnp.float32), ffn_gain).astype(jnp.bfloat16)
     width = normed.shape[1]
+    if n_sp == 4 and n_tp <= 4 and tok_rows == 128 and w_gate.shape[2] <= 256 and w_gate.shape[0] <= 8 and tok_rows * width <= 128 * 2048:
+        expert_mix = dense_experts(normed, routes, route_weight, w_gate, w_up, w_down)
+        return (residual.astype(jnp.float32) + rms_scale(expert_mix, post_gain)).astype(jnp.bfloat16)
     local_experts = w_gate.shape[0]
     n_experts = local_experts * n_sp
     slot_total = n_experts * CAP

time: 290 us -> 166 us (0.57)
  waiting for transfers between devices: 181 us -> 8.14 us
  Pallas kernels: 0 us -> 134 us
  blocking collectives: 37.6 us -> 0 us
  matrix products: 27 us -> 3.24 us
  local copies, waits for them, and re-layouts: 17.3 us -> 3.19 us
  between operations: 13.6 us -> 0.17 us
  other arithmetic: 4.92 us -> 8.67 us
    pallas_call x0 -> x1, Pallas kernels: none -> 134 us  [dense_experts(): pl.pallas_call(functools.partial(layer_kernel, n_tp, cuts), out_shape=jax...]
    all_gather x1 -> x0, waiting for transfers between devices: 88.8 us -> none  [per_device(): arrived = lax.all_gather(at_owner[:, None], 'tp', axis=1, tiled=True)]
    reduce_scatter x1 -> x0, waiting for transfers between devices: 83.8 us -> none  [per_device(): lax.psum_scatter(terms.reshape(1 * lax.axis_size('tp'), n_sp, local_exper...]
    all_to_all x2 -> x0, blocking collectives: 37.6 us -> none  [the longest x1 19.3 us: per_device(): lax.all_to_all(results, 'sp', split_axis=0, concat_axis=0, tiled=True)]
    dot_general x4 -> x0, matrix products: 23.7 us -> none  [the longest x1 14 us: per_device(): jnp.einsum('sklcf,lfd->kslcd', activated, w_down, preferred_element_type=...]
    convert_element_type x2 -> x0, local copies, waits for them, and re-layouts: 13 us -> none  [per_device(): terms.reshape(1 * lax.axis_size('tp'), n_sp, local_experts * CAP, width)]
  transfers between devices with their start and end apart: 4 -> 2, of which waited for: 3 -> 1; matrix products, arithmetic and copies ran while one was open for 1% -> 2% of each run, Pallas kernels for 0% -> 0%
where the time goes in v2:
time: 166 us
  Pallas kernels  134 us (81%)
  other arithmetic  8.67 us (5%)
  starting transfers between devices  8.2 us (5%)
  waiting for transfers between devices  8.14 us (5%)
  matrix products  3.24 us (2%)
  local copies, waits for them, and re-layouts  3.19 us (2%)
    pallas_call x1, Pallas kernels, dense_experts(): pl.pallas_call(functools.partial(layer_kernel, n_tp, cuts), out_shape=jax...  134 us
    all_to_all x1, waiting for transfers between devices, per_device(): lax.all_to_all(mixed_rows, 'tp', split_axis=0, concat_axis=1, tiled=True)  8.14 us
    all_to_all x1, starting transfers between devices, per_device(): lax.all_to_all(mixed_rows, 'tp', split_axis=0, concat_axis=1, tiled=True)  5.82 us
  transfers between devices with their start and end apart: 2, of which 1 were waited for; matrix products, arithmetic and copies ran while one was open for 2% of the time, Pallas kernels for 0%

profile of v2, /device:TPU:0, one launch (start us, length us, event | category | flops | bytes accessed | tf_op | source)
XLA Modules:
  0.0 165.7 jit_solution(6819905909078352624)
XLA Ops:
  0.0 0.0 copy-start
  0.0 0.8 slice.58
  0.8 2.4 %collective-permute-start = (bf16[15,256]{1,0:T(8,128)(2,1)S(1)}, bf16[15,256]{1,0:T(8,128)(2,1)S(1)}, u32[]{:S(2)}, u32[]{:S(2)}) collective-permute-start(bf16[15,256]{1,0:T(8,128)(2,1)S(1)} %slice.58), channel_id=1, source_target_pairs={{0,4},{4,8},{8,12},{1,5},{5,9},{9,13},{2,6},{6,10},{10,14},{3,7},{... | collective-permute-start | bytes 23048 | tf_op jit(solution)/shard_map/ppermute | solution.py:26
  3.2 0.8 copy.15
  4.0 0.1 eq.158
  4.1 0.1 eq.154
  4.3 0.6 reduce-window.6
  4.9 0.2 slice_reduce_fusion
  5.1 0.1 fusion.15
  5.2 0.7 mul.85
  5.9 0.1 reshape.107
  6.1 0.1 copy.18
  6.1 0.1 pad.2.clone
  6.2 0.0 collective-permute-done
  6.2 1.0 maximum_convert_fusion
  7.3 0.0 copy-start.5
  7.3 0.0 copy-start.6
  7.3 1.5 fusion.11
  8.8 0.0 copy-start.1
  8.8 0.0 copy-start.2
  8.8 5.8 %all-to-all-start = ((bf16[4,128,256]{2,1,0:T(8,128)(2,1)}), bf16[4,128,256]{2,1,0:T(8,128)(2,1)S(1)}, u32[]{:S(2)}, u32[]{:S(2)}) async-start(bf16[4,128,256]{2,1,0:T(8,128)(2,1)} %bitcast), calls=%async_computation | async-start | bytes 524288 | tf_op jit(solution)/shard_map/all_to_all | solution.py:450
  14.6 0.0 copy-done.5
  14.6 0.0 copy-done.6
  14.6 0.7 maximum_bitcast_fusion.meta_ref
  15.3 8.1 %all-to-all-done = bf16[4,128,256]{2,1,0:T(8,128)(2,1)S(1)} async-done(((bf16[4,128,256]{2,1,0:T(8,128)(2,1)}), bf16[4,128,256]{2,1,0:T(8,128)(2,1)S(1)}, u32[]{:S(2)}, u32[]{:S(2)}) %all-to-all-start) | async-done | bytes 262176 | tf_op jit(solution)/shard_map/all_to_all | solution.py:450
  23.4 0.0 copy-done
  23.4 0.2 fusion.1
  23.7 0.0 copy-start.3
  23.7 0.2 copy.14
  23.9 3.0 %multiply_reduce_fusion = (f32[128]{0:T(128)S(1)}, f32[128,2048]{1,0:T(8,128)S(1)}) fusion(bf16[128,1024]{0,1:T(8,128)(2,1)S(1)} %bitcast.31, bf16[1024,2048]{1,0:T(8,128)(2,1)} %param.17), kind=kOutput, calls=%fused_computation.15 | convolution fusion | flops 537395072 | bytes 5505536 | tf_op jit(solution)/shard_map/dot_general | solution.py:461
  26.9 0.0 copy-done.1
  26.9 0.0 copy-done.2
  26.9 0.4 fusion.4
  27.3 0.0 copy-done.3
  27.3 1.0 fusion.6.row_ref
  28.3 0.0 copy-start.4
  28.3 134.0 %routed_experts.1 = bf16[128,2048]{1,0:T(8,128)(2,1)} custom-call(bf16[128,2048]{1,0:T(8,128)(2,1)} %fusion.6.row_ref, f32[8,128]{1,0:T(8,128)} %maximum_bitcast_fusion.meta_ref, bf16[8,2048,256]{2,1,0:T(8,128)(2,1)} %wg_ref.1, bf16[8,2048,256]{2,1,0:T(8,128)(2,1)} %wu_ref.1, bf16[8,256,2048]{2,1,0:T(8,128)(2,1)} %wd_ref.1), custom_call_target="tpu_custom_call" | custom-call | tf_op jit(solution)/shard_map/routed_experts/pallas_call | solution.py:372
  162.3 1.2 fusion.2
  163.6 0.0 copy-done.4
  163.6 2.1 %fusion.7 = bf16[128,2048]{1,0:T(8,128)(2,1)} fusion(bf16[128,2048]{1,0:T(8,128)(2,1)} %routed_experts.1, bf16[128,2048]{1,0:T(8,128)(2,1)S(1)} %get-tuple-element.6, f32[2048]{0:T(1024)S(1)} %copy-done.4, f32[128]{0:T(128)S(1)} %add_rsqrt_fusion), kind=kLoop, calls=%fused_computation.13 | loop fusion | flops 1572864 | bytes 1581568 | tf_op jit(solution)/shard_map/convert_element_type | solution.py:467
  (12 shorter events, 0.1 us)
Async XLA Ops:
  0.0 23.4 %copy-start = (bf16[4,256,256]{2,1,0:T(8,128)(2,1)S(1)}, bf16[4,256,256]{2,1,0:T(8,128)(2,1)}, u32[]{:S(2)}) copy-start(bf16[4,256,256]{2,1,0:T(8,128)(2,1)} %param.15) | copy-start | bytes 1572868
  0.8 5.5 %collective-permute-start = (bf16[15,256]{1,0:T(8,128)(2,1)S(1)}, bf16[15,256]{1,0:T(8,128)(2,1)S(1)}, u32[]{:S(2)}, u32[]{:S(2)}) collective-permute-start(bf16[15,256]{1,0:T(8,128)(2,1)S(1)} %slice.58), channel_id=1, source_target_pairs={{0,4},{4,8},{8,12},{1,5},{5,9},{9,13},{2,6},{6,10},{10,14},{3,7},{... | collective-permute-start | bytes 23048 | tf_op jit(solution)/shard_map/ppermute | solution.py:26
  7.3 7.3 %copy-start.5 = (s32[128,2]{0,1:T(2,128)S(1)}, s32[128,2]{0,1:T(2,128)}, u32[]{:S(2)}) copy-start(s32[128,2]{0,1:T(2,128)} %param.23) | copy-start | bytes 3076
  7.3 7.3 %copy-start.6 = (f32[128,2]{0,1:T(2,128)S(1)}, f32[128,2]{0,1:T(2,128)}, u32[]{:S(2)}) copy-start(f32[128,2]{0,1:T(2,128)} %param.24) | copy-start | bytes 3076
  8.8 18.1 %copy-start.1 = (bf16[128,2048]{1,0:T(8,128)(2,1)S(1)}, bf16[128,2048]{1,0:T(8,128)(2,1)}, u32[]{:S(2)}) copy-start(bf16[128,2048]{1,0:T(8,128)(2,1)} %param.13) | copy-start | bytes 1572868
  8.8 18.1 %copy-start.2 = (f32[2048]{0:T(1024)S(1)}, f32[2048]{0:T(1024)}, u32[]{:S(2)}) copy-start(f32[2048]{0:T(1024)} %param.18) | copy-start | bytes 24580
  8.8 14.6 %all-to-all-start = ((bf16[4,128,256]{2,1,0:T(8,128)(2,1)}), bf16[4,128,256]{2,1,0:T(8,128)(2,1)S(1)}, u32[]{:S(2)}, u32[]{:S(2)}) async-start(bf16[4,128,256]{2,1,0:T(8,128)(2,1)} %bitcast), calls=%async_computation | async-start | bytes 524288 | tf_op jit(solution)/shard_map/all_to_all | solution.py:450
  23.7 3.6 %copy-start.3 = (f32[2048]{0:T(1024)S(1)}, f32[2048]{0:T(1024)}, u32[]{:S(2)}) copy-start(f32[2048]{0:T(1024)} %param.19) | copy-start | bytes 24580
  28.3 135.3 %copy-start.4 = (f32[2048]{0:T(1024)S(1)}, f32[2048]{0:T(1024)}, u32[]{:S(2)}) copy-start(f32[2048]{0:T(1024)} %param.25) | copy-start | bytes 24580

commit v3 on v2

--- a/solution.py
+++ b/solution.py
@@ -39,6 +39,7 @@
 
 SLOT = 16
 Y_FIRST = 16
+Z_PART = 64
 MESH = pl.DeviceIdType.MESH
 
 
@@ -141,13 +142,14 @@
     for number, by in enumerate(others):
         meta_copy(number, by).start()
     push(yes, sp, tp, 0, 2)
-    push(yes, sp, tp, 1, 0)
-    push(yes, sp, tp, 1, 1)
-    push(yes, sp, tp, 1, 2)
+    for part in (1, 2):
+        push(yes, sp, tp, part, 0)
+        push(yes, sp, tp, part, 1)
+        push(yes, sp, tp, part, 2)
     push(yes, sp, tp, 0, 0)
     push(yes, sp, tp, 0, 1)
-    push(yes, sp, tp, 0, 3)
-    push(yes, sp, tp, 1, 3)
+    for part in (0, 1, 2):
+        push(yes, sp, tp, part, 3)
     for e in range(min(buffers, local_experts)):
         for c in weight_copies(e):
             c.start()
@@ -158,39 +160,48 @@
     select(sp, tp)
     for number, by in enumerate(others):
         meta_copy(number, by).wait()
+
+    def sides(dist):
+        if dist == 0:
+            return ((tp, yes),)
+        return ((tp - dist, tp >= dist), (tp + dist, tp + dist < n_tp))
+
+    def over_y(dist):
+        for t, cond in sides(dist):
+            for part in (1, 2):
+                pl.when(cond)(functools.partial(arrived, y_other, t, part))
+                push(cond, y_other, t, part, 3)
+            pl.when(cond)(functools.partial(select, y_other, t))
+
+    def cross(s, t):
+        for part in (0, 1, 2):
+            arrived(s, t, part)
+        select(s, t)
+
+    def over_core(s, dist):
+        for t, cond in sides(dist):
+            pl.when(cond)(functools.partial(cross, s, t))
+
+    far_core = yo * 2 + (1 - core)
     for dist in range(1, n_tp):
-        for s, part in ((sp, 1), (sp, 0), (y_other, 0)):
-            for way in (0, 1):
-                t = tp - dist if way == 0 else tp + dist
-                cond = t >= 0 if way == 0 else t < n_tp
+        for s, part in ((sp, 1), (sp, 2), (sp, 0), (y_other, 0)):
+            for way, (t, cond) in enumerate(sides(dist)):
                 pl.when(cond)(functools.partial(arrived, s, t, part))
                 push(cond, s, t, part, way)
-                if part == 1:
+                if part:
                     push(cond, s, t, part, 2)
                 push(cond, s, t, part, 3)
-        if dist == 1:
-            arrived(y_other, tp, 1)
-            push(yes, y_other, tp, 1, 3)
-            select(y_other, tp)
-        for way in (0, 1):
-            t = tp - dist if way == 0 else tp + dist
-            cond = t >= 0 if way == 0 else t < n_tp
+        for t, cond in sides(dist):
             pl.when(cond)(functools.partial(select, sp, t))
-    for dist in range(1, n_tp):
-        for way in (0, 1):
-            t = tp - dist if way == 0 else tp + dist
-            cond = t >= 0 if way == 0 else t < n_tp
-            pl.when(cond)(functools.partial(arrived, y_other, t, 1))
-            push(cond, y_other, t, 1, 3)
-            pl.when(cond)(functools.partial(select, y_other, t))
-    for s in (c_other, yo * 2 + (1 - core)):
-        def cross(t, carry, s=s):
-            for part in (0, 1):
-                arrived(s, t, part)
-            select(s, t)
-            return carry
-
-        lax.fori_loop(0, n_tp, cross, 0)
+        over_core(c_other, dist - 1)
+        over_y(dist - 1)
+        if dist > 1:
+            over_core(far_core, dist - 2)
+    over_core(c_other, n_tp - 1)
+    if n_tp > 1:
+        over_core(far_core, n_tp - 2)
+    over_y(n_tp - 1)
+    over_core(far_core, n_tp - 1)
     for cond, s, t, part, way in sent:
         pl.when(cond)(lambda s=s, t=t, part=part, way=way: copy(s, t, part, way).wait_send())
 
@@ -226,8 +237,8 @@
         return lax.dot_general(picks[s, t], term, (((0,), (0,)), ((), ())),
                                preferred_element_type=jnp.float32)
 
-    (a0, an), (b0, bn) = cuts
-    rows_a, rows_b = pl.ds(a0, an), pl.ds(b0, bn)
+    rows_of = [pl.ds(first, count) for first, count in cuts]
+    rows_a = rows_of[0]
     ups, downs = (grp, sp, tp + 1), (grp, sp, tp - 1)
     up_ok, down_ok = tp + 1 < n_tp, tp > 0
 
@@ -257,11 +268,13 @@
             t = tp + side * dist
             order.append((jnp.logical_and(t >= 0, t < n_tp), t, side, dist))
 
-    def y_copy_b(t):
-        return remote(work.at[yo, t, rows_b], yb.at[t], ysend.at[t], yrecv.at[t], (grp, y_other, tp))
+    def y_copy_b(part, t):
+        rows = rows_of[part]
+        return remote(work.at[yo, t, rows], yb.at[t, rows], ysend.at[part, t], yrecv.at[part, t],
+                      (grp, y_other, tp))
 
     def y_copy_a():
-        return remote(work.at[yo, tp, rows_a], ya, ysend.at[n_tp], yrecv.at[n_tp], (grp, y_other, tp))
+        return remote(work.at[yo, tp, rows_a], ya, ysend.at[0, 0], yrecv.at[0, 0], (grp, y_other, tp))
 
     def local(y, t):
         s = y * 2 + core
@@ -275,21 +288,23 @@
 
         lax.fori_loop(0, width // chunk, body, 0)
 
+    def z_ends(part, y, t, slot):
+        rows = rows_of[part]
+        if part:
+            return work.at[y, t, rows], zb.at[slot, rows], bsend.at[part, t], brecv.at[part, slot]
+        return work.at[y, t, rows], za.at[y, slot], asend.at[y, t], arecv.at[y, slot]
+
     def z_copy(part, y, t, side):
-        buf, ss, rs, rows = ((za, asend, arecv, rows_a), (zb, bsend, brecv, rows_b))[part]
         if side == 1:
             slot, target = t, ups
         else:
-            slot = jnp.where(t == tp - 1, n_tp, t)
-            target = downs
-        row = y if part == 0 else 0
-        return remote(work.at[y, t, rows], buf.at[row, slot], ss.at[row, t], rs.at[row, slot], target)
+            slot, target = jnp.where(t == tp - 1, n_tp, t), downs
+        return remote(*z_ends(part, y, t, slot), target)
 
     def take_z(part, y, t, slot):
-        buf, ss, rs, rows = ((za, asend, arecv, rows_a), (zb, bsend, brecv, rows_b))[part]
-        row = y if part == 0 else 0
-        remote(work.at[y, t, rows], buf.at[row, slot], ss.at[row, t], rs.at[row, slot], ups).wait_recv()
-        add_into(work.at[y, t, rows], buf.at[row, slot])
+        remote(*z_ends(part, y, t, slot), ups).wait_recv()
+        dst, src = z_ends(part, y, t, slot)[:2]
+        add_into(dst, src)
 
     def z_step(part, y, t, side):
         inner = tp > 0 if side == 1 else tp + 1 < n_tp
@@ -308,21 +323,25 @@
                 @pl.when(ok)
                 def _(t=t):
                     local(yo, t)
-                    y_copy_b(t).start()
+                    y_copy_b(1, t).start()
+                    y_copy_b(2, t).start()
     for ok, t, side, dist in order:
         @pl.when(ok)
         def _(t=t, side=side, dist=dist):
             local(yy, t)
-            y_copy_b(t).wait_recv()
-            add_into(work.at[yy, t, rows_b], yb.at[t])
             if dist:
-                z_step(1, yy, t, side)
                 z_step(0, yo, t, side)
                 z_step(0, yy, t, side)
+            for part in (1, 2):
+                y_copy_b(part, t).wait_recv()
+                add_into(work.at[yy, t, rows_of[part]], yb.at[t, rows_of[part]])
+                if dist:
+                    z_step(part, yy, t, side)
     z_end(0, yo)
     y_copy_a().start()
     z_end(0, yy)
     z_end(1, yy)
+    z_end(2, yy)
     y_copy_a().wait_recv()
     add_into(work.at[yy, tp, rows_a], ya)
     last = pltpu.make_async_copy(work.at[yy, tp], out_ref, own.at[0, 0])
@@ -334,11 +353,13 @@
         def _(t=t, side=side, dist=dist):
             core_copy(yo, t).wait_send()
             core_copy(yy, t).wait_send()
-            y_copy_b(t).wait_send()
+            y_copy_b(1, t).wait_send()
+            y_copy_b(2, t).wait_send()
             if dist:
                 z_copy(0, yo, t, side).wait_send()
                 z_copy(0, yy, t, side).wait_send()
                 z_copy(1, yy, t, side).wait_send()
+                z_copy(2, yy, t, side).wait_send()
 
 
 def add_into(dst, src):
@@ -363,8 +384,8 @@
     rank = jnp.sum((jnp.cumsum(onehot, axis=0) - onehot) * onehot, axis=1).reshape(tok, TOP)
     place = (routes * SLOT + rank).astype(jnp.float32)
     meta = jnp.concatenate([place, route_weight, jnp.zeros((tok, 8 - 2 * TOP), jnp.float32)], axis=1).T
-    cuts = ((0, Y_FIRST), (Y_FIRST, tok - Y_FIRST))
-    an, bn = cuts[0][1], cuts[1][1]
+    cuts = ((0, Y_FIRST), (Y_FIRST, Z_PART), (Y_FIRST + Z_PART, tok - Y_FIRST - Z_PART))
+    an = cuts[0][1]
     vmem, hbm = pl.BlockSpec(memory_space=pltpu.VMEM), pl.BlockSpec(memory_space=pl.ANY)
     kind = normed.dtype
     slots, buffers = local_experts * SLOT, min(4, local_experts)
@@ -386,11 +407,11 @@
             pltpu.VMEM((2, n_tp, tok, width), kind),
             pltpu.VMEM((2, n_tp, tok, width), kind),
             pltpu.VMEM((2, n_tp + 1, an, width), kind),
-            pltpu.VMEM((1, n_tp + 1, bn, width), kind),
+            pltpu.VMEM((n_tp + 1, tok, width), kind),
             pltpu.VMEM((an, width), kind),
-            pltpu.VMEM((n_tp, bn, width), kind),
-            dma((4, n_tp, 2, 4)),
-            dma((4, n_tp, 2)),
+            pltpu.VMEM((n_tp, tok, width), kind),
+            dma((4, n_tp, 3, 4)),
+            dma((4, n_tp, 3)),
             dma((4 * n_tp - 1,)),
             dma((4 * n_tp - 1,)),
             dma((3, buffers)),
@@ -398,10 +419,10 @@
             dma((2, n_tp)),
             dma((2, n_tp)),
             dma((2, n_tp + 1)),
-            dma((1, n_tp)),
-            dma((1, n_tp + 1)),
-            dma((n_tp + 1,)),
-            dma((n_tp + 1,)),
+            dma((3, n_tp)),
+            dma((3, n_tp + 1)),
+            dma((3, n_tp)),
+            dma((3, n_tp)),
             dma((2, max(2, n_tp))),
         ],
         compiler_params=pltpu.CompilerParams(

time: 166 us -> 156 us (0.940)
  Pallas kernels: 134 us -> 124 us
    pallas_call x1, Pallas kernels: 134 us -> 124 us  [dense_experts(): pl.pallas_call(functools.partial(layer_kernel, n_tp, cuts), out_shape=jax...]
where the time goes in v3:
time: 156 us; the launch traced here: 155 us
  Pallas kernels  124 us (79%)
  other arithmetic  8.67 us (6%)
  starting transfers between devices  8.2 us (5%)
  waiting for transfers between devices  8.14 us (5%)
  matrix products  3.24 us (2%)
  local copies, waits for them, and re-layouts  3.19 us (2%)
    pallas_call x1, Pallas kernels, dense_experts(): pl.pallas_call(functools.partial(layer_kernel, n_tp, cuts), out_shape=jax...  124 us
    all_to_all x1, waiting for transfers between devices, per_device(): lax.all_to_all(mixed_rows, 'tp', split_axis=0, concat_axis=1, tiled=True)  8.14 us
    all_to_all x1, starting transfers between devices, per_device(): lax.all_to_all(mixed_rows, 'tp', split_axis=0, concat_axis=1, tiled=True)  5.82 us
  transfers between devices with their start and end apart: 2, of which 1 were waited for; matrix products, arithmetic and copies ran while one was open for 2% of the time, Pallas kernels for 0%

profile of v3, /device:TPU:0, one launch (start us, length us, event | category | flops | bytes accessed | tf_op | source)
XLA Modules:
  0.0 155.2 jit_solution(10008452203089030645)
XLA Ops:
  0.0 0.0 copy-start
  0.0 0.8 slice.58
  0.8 2.4 %collective-permute-start = (bf16[15,256]{1,0:T(8,128)(2,1)S(1)}, bf16[15,256]{1,0:T(8,128)(2,1)S(1)}, u32[]{:S(2)}, u32[]{:S(2)}) collective-permute-start(bf16[15,256]{1,0:T(8,128)(2,1)S(1)} %slice.58), channel_id=1, source_target_pairs={{0,4},{4,8},{8,12},{1,5},{5,9},{9,13},{2,6},{6,10},{10,14},{3,7},{... | collective-permute-start | bytes 23048 | tf_op jit(solution)/shard_map/ppermute | solution.py:26
  3.2 0.8 copy.15
  4.0 0.1 eq.158
  4.1 0.1 eq.154
  4.3 0.6 reduce-window.6
  4.9 0.2 slice_reduce_fusion
  5.1 0.1 fusion.15
  5.2 0.7 mul.85
  5.9 0.1 reshape.107
  6.1 0.1 copy.18
  6.1 0.1 pad.2.clone
  6.2 0.0 collective-permute-done
  6.2 1.0 maximum_convert_fusion
  7.3 0.0 copy-start.5
  7.3 0.0 copy-start.6
  7.3 1.5 fusion.11
  8.8 0.0 copy-start.1
  8.8 0.0 copy-start.2
  8.8 5.8 %all-to-all-start = ((bf16[4,128,256]{2,1,0:T(8,128)(2,1)}), bf16[4,128,256]{2,1,0:T(8,128)(2,1)S(1)}, u32[]{:S(2)}, u32[]{:S(2)}) async-start(bf16[4,128,256]{2,1,0:T(8,128)(2,1)} %bitcast), calls=%async_computation | async-start | bytes 524288 | tf_op jit(solution)/shard_map/all_to_all | solution.py:471
  14.6 0.0 copy-done.5
  14.6 0.0 copy-done.6
  14.6 0.7 maximum_bitcast_fusion.meta_ref
  15.3 8.1 %all-to-all-done = bf16[4,128,256]{2,1,0:T(8,128)(2,1)S(1)} async-done(((bf16[4,128,256]{2,1,0:T(8,128)(2,1)}), bf16[4,128,256]{2,1,0:T(8,128)(2,1)S(1)}, u32[]{:S(2)}, u32[]{:S(2)}) %all-to-all-start) | async-done | bytes 262176 | tf_op jit(solution)/shard_map/all_to_all | solution.py:471
  23.4 0.0 copy-done
  23.4 0.2 fusion.1
  23.7 0.0 copy-start.3
  23.7 0.2 copy.14
  23.9 3.0 %multiply_reduce_fusion = (f32[128]{0:T(128)S(1)}, f32[128,2048]{1,0:T(8,128)S(1)}) fusion(bf16[128,1024]{0,1:T(8,128)(2,1)S(1)} %bitcast.31, bf16[1024,2048]{1,0:T(8,128)(2,1)} %param.17), kind=kOutput, calls=%fused_computation.15 | convolution fusion | flops 537395072 | bytes 5505536 | tf_op jit(solution)/shard_map/dot_general | solution.py:482
  26.9 0.0 copy-done.1
  26.9 0.0 copy-done.2
  26.9 0.4 fusion.4
  27.3 0.0 copy-done.3
  27.3 1.0 fusion.6.row_ref
  28.3 0.0 copy-start.4
  28.3 123.6 %routed_experts.1 = bf16[128,2048]{1,0:T(8,128)(2,1)} custom-call(bf16[128,2048]{1,0:T(8,128)(2,1)} %fusion.6.row_ref, f32[8,128]{1,0:T(8,128)} %maximum_bitcast_fusion.meta_ref, bf16[8,2048,256]{2,1,0:T(8,128)(2,1)} %wg_ref.1, bf16[8,2048,256]{2,1,0:T(8,128)(2,1)} %wu_ref.1, bf16[8,256,2048]{2,1,0:T(8,128)(2,1)} %wd_ref.1), custom_call_target="tpu_custom_call" | custom-call | tf_op jit(solution)/shard_map/routed_experts/pallas_call | solution.py:393
  151.9 1.2 fusion.2
  153.1 0.0 copy-done.4
  153.1 2.1 %fusion.7 = bf16[128,2048]{1,0:T(8,128)(2,1)} fusion(bf16[128,2048]{1,0:T(8,128)(2,1)} %routed_experts.1, bf16[128,2048]{1,0:T(8,128)(2,1)S(1)} %get-tuple-element.6, f32[2048]{0:T(1024)S(1)} %copy-done.4, f32[128]{0:T(128)S(1)} %add_rsqrt_fusion), kind=kLoop, calls=%fused_computation.13 | loop fusion | flops 1572864 | bytes 1581568 | tf_op jit(solution)/shard_map/convert_element_type | solution.py:488
  (12 shorter events, 0.1 us)
Async XLA Ops:
  0.0 23.4 %copy-start = (bf16[4,256,256]{2,1,0:T(8,128)(2,1)S(1)}, bf16[4,256,256]{2,1,0:T(8,128)(2,1)}, u32[]{:S(2)}) copy-start(bf16[4,256,256]{2,1,0:T(8,128)(2,1)} %param.15) | copy-start | bytes 1572868
  0.8 5.5 %collective-permute-start = (bf16[15,256]{1,0:T(8,128)(2,1)S(1)}, bf16[15,256]{1,0:T(8,128)(2,1)S(1)}, u32[]{:S(2)}, u32[]{:S(2)}) collective-permute-start(bf16[15,256]{1,0:T(8,128)(2,1)S(1)} %slice.58), channel_id=1, source_target_pairs={{0,4},{4,8},{8,12},{1,5},{5,9},{9,13},{2,6},{6,10},{10,14},{3,7},{... | collective-permute-start | bytes 23048 | tf_op jit(solution)/shard_map/ppermute | solution.py:26
  7.3 7.3 %copy-start.5 = (s32[128,2]{0,1:T(2,128)S(1)}, s32[128,2]{0,1:T(2,128)}, u32[]{:S(2)}) copy-start(s32[128,2]{0,1:T(2,128)} %param.23) | copy-start | bytes 3076
  7.3 7.3 %copy-start.6 = (f32[128,2]{0,1:T(2,128)S(1)}, f32[128,2]{0,1:T(2,128)}, u32[]{:S(2)}) copy-start(f32[128,2]{0,1:T(2,128)} %param.24) | copy-start | bytes 3076
  8.8 18.1 %copy-start.1 = (bf16[128,2048]{1,0:T(8,128)(2,1)S(1)}, bf16[128,2048]{1,0:T(8,128)(2,1)}, u32[]{:S(2)}) copy-start(bf16[128,2048]{1,0:T(8,128)(2,1)} %param.13) | copy-start | bytes 1572868
  8.8 18.1 %copy-start.2 = (f32[2048]{0:T(1024)S(1)}, f32[2048]{0:T(1024)}, u32[]{:S(2)}) copy-start(f32[2048]{0:T(1024)} %param.18) | copy-start | bytes 24580
  8.8 14.6 %all-to-all-start = ((bf16[4,128,256]{2,1,0:T(8,128)(2,1)}), bf16[4,128,256]{2,1,0:T(8,128)(2,1)S(1)}, u32[]{:S(2)}, u32[]{:S(2)}) async-start(bf16[4,128,256]{2,1,0:T(8,128)(2,1)} %bitcast), calls=%async_computation | async-start | bytes 524288 | tf_op jit(solution)/shard_map/all_to_all | solution.py:471
  23.7 3.6 %copy-start.3 = (f32[2048]{0:T(1024)S(1)}, f32[2048]{0:T(1024)}, u32[]{:S(2)}) copy-start(f32[2048]{0:T(1024)} %param.19) | copy-start | bytes 24580
  28.3 124.8 %copy-start.4 = (f32[2048]{0:T(1024)S(1)}, f32[2048]{0:T(1024)}, u32[]{:S(2)}) copy-start(f32[2048]{0:T(1024)} %param.25) | copy-start | bytes 24580

commit v4 on v3

--- a/solution.py
+++ b/solution.py
@@ -45,6 +45,146 @@
 
 def coords():
     return lax.axis_index("grp"), lax.axis_index("sp"), lax.axis_index("tp")
+
+
+def exchange_kernel(n_tp, pool_ref, out_ref, send, recv, hsend, hrecv, own):
+    grp, sp, tp = coords()
+    seg_rows = pool_ref.shape[0]
+    tok, reach = seg_rows // n_tp, SLOT
+    first = tp == 0
+    others = [(a, b) for a in range(4) for b in range(n_tp) if (a, b) != (0, 0)]
+    barrier = pltpu.get_barrier_semaphore()
+    for by in others:
+        target = (grp, (sp + by[0]) % 4, (tp + by[1]) % n_tp)
+        pl.semaphore_signal(barrier, inc=1, device_id=target, device_id_type=MESH)
+
+    def ends(to, whole, chan):
+        if whole:
+            at = pl.multiple_of(to * tok - reach, reach)
+            return pool_ref.at[pl.ds(at, tok + reach)], out_ref.at[chan]
+        return pool_ref.at[pl.ds(0, tok)], out_ref.at[chan, pl.ds(reach, tok)]
+
+    def main(by, whole):
+        to = (tp + by) % n_tp
+        src, dst = ends(to, whole, tp)
+        return pltpu.make_async_remote_copy(
+            src_ref=src, dst_ref=dst, send_sem=send.at[by], recv_sem=recv.at[tp],
+            device_id=(grp, sp, to), device_id_type=MESH)
+
+    def arrival(by, whole):
+        chan = (tp + by) % n_tp
+        src, dst = ends(1 if whole else 0, whole, chan)
+        return pltpu.make_async_remote_copy(
+            src_ref=src, dst_ref=dst, send_sem=send.at[by], recv_sem=recv.at[chan],
+            device_id=(grp, sp, chan), device_id_type=MESH)
+
+    def halo(chan):
+        return pltpu.make_async_remote_copy(
+            src_ref=pool_ref.at[pl.ds(seg_rows - reach, reach)],
+            dst_ref=out_ref.at[chan, pl.ds(0, reach)],
+            send_sem=hsend.at[0], recv_sem=hrecv.at[chan],
+            device_id=(grp, sp + 1, 0), device_id_type=MESH)
+
+    def kept(whole):
+        src, dst = ends(tp, whole, tp)
+        return pltpu.make_async_copy(src, dst, own.at[0])
+
+    pl.semaphore_wait(barrier, len(others))
+    rest = jnp.logical_not(first)
+    has_next = sp + 1 < 4
+    pl.when(has_next)(lambda: halo(tp).start())
+    for by in range(1, n_tp):
+        to_first = (tp + by) % n_tp == 0
+        pl.when(to_first)(lambda by=by: main(by, False).start())
+        pl.when(jnp.logical_not(to_first))(lambda by=by: main(by, True).start())
+    pl.when(first)(lambda: kept(False).start())
+    pl.when(rest)(lambda: kept(True).start())
+
+    @pl.when(jnp.logical_and(first, sp == 0))
+    def _():
+        for chan in range(n_tp):
+            out_ref[chan, pl.ds(0, reach)] = jnp.zeros((reach, out_ref.shape[2]), out_ref.dtype)
+
+    pl.when(first)(lambda: kept(False).wait())
+    pl.when(rest)(lambda: kept(True).wait())
+    for by in range(1, n_tp):
+        pl.when(first)(lambda by=by: arrival(by, False).wait_recv())
+        pl.when(rest)(lambda by=by: arrival(by, True).wait_recv())
+
+    @pl.when(jnp.logical_and(first, sp > 0))
+    def _():
+        for chan in range(n_tp):
+            halo(chan).wait_recv()
+
+    pl.when(has_next)(lambda: halo(tp).wait_send())
+    for by in range(1, n_tp):
+        to_first = (tp + by) % n_tp == 0
+        pl.when(to_first)(lambda by=by: main(by, False).wait_send())
+        pl.when(jnp.logical_not(to_first))(lambda by=by: main(by, True).wait_send())
+
+
+def mixed_tokens(pool_input, pool_weight, pool_scale, n_tp):
+    seg_rows, channels = pool_input.shape
+    tok = seg_rows // n_tp
+    vmem = pl.BlockSpec(memory_space=pltpu.VMEM)
+    dma = pltpu.SemaphoreType.DMA
+    rows = pl.pallas_call(
+        functools.partial(exchange_kernel, n_tp),
+        out_shape=jax.ShapeDtypeStruct((n_tp, tok + SLOT, channels), pool_input.dtype),
+        in_specs=[vmem],
+        out_specs=vmem,
+        scratch_shapes=[dma((n_tp,)), dma((n_tp,)), dma((1,)), dma((n_tp,)), dma((1,))],
+        compiler_params=pltpu.CompilerParams(collective_id=1, has_side_effects=True),
+        name="pool_exchange",
+    )(pool_input)
+    start = (lax.axis_index("sp") * n_tp + lax.axis_index("tp")) * tok
+    count = start + lax.broadcasted_iota(jnp.int32, (tok, 1), 0) + 1
+    pooled = []
+    for group, window in enumerate(pool_windows):
+        held = rows[group].astype(jnp.float32)
+        total = held[SLOT:]
+        for offset in range(1, window):
+            total = total + held[SLOT - offset : SLOT - offset + tok]
+        divisor = jnp.minimum(count, window).astype(jnp.float32)
+        mixed = (total / divisor - held[SLOT:]).astype(jnp.bfloat16)
+        product = jnp.dot(mixed, pool_weight[group], preferred_element_type=jnp.float32)
+        scale = pool_scale[group * GROUP_DIM : (group + 1) * GROUP_DIM]
+        pooled.append((product * scale).astype(jnp.bfloat16))
+    return jnp.concatenate(pooled, axis=1)
+
+
+def routed_pool(pool_input, pool_weight, pool_scale):
+    n_tp = lax.axis_size("tp")
+    seg_rows, channels = pool_input.shape
+    last_rows = pool_input[seg_rows - reach_back :]
+    before = passed_along(last_rows, "sp", 1)
+    extended = jnp.concatenate([before, pool_input], axis=0).astype(jnp.float32)
+    first_chan = lax.axis_index("tp") * channels
+    chan_group = (first_chan + lax.iota(jnp.int32, channels)) // GROUP_DIM
+    positions = lax.axis_index("sp") * seg_rows + lax.iota(jnp.int32, seg_rows)
+    window = jnp.zeros((channels,), jnp.int32)
+    for group_level, win_len in enumerate(pool_windows):
+        window = jnp.where(chan_group == group_level, win_len, window)
+    running = jnp.zeros((seg_rows, channels), jnp.float32)
+    window_sum = running
+    for offset in range(pool_windows[-1]):
+        running = running + extended[reach_back - offset : reach_back - offset + seg_rows]
+        if offset + 1 in pool_windows:
+            window_sum = jnp.where(window[None, :] == offset + 1, running, window_sum)
+    divisor = jnp.minimum(positions[:, None] + 1, window[None, :]).astype(jnp.float32)
+    mixed_rows = (window_sum / divisor - extended[reach_back:]).astype(jnp.bfloat16)
+    token_mixed = lax.all_to_all(mixed_rows, "tp", split_axis=0, concat_axis=1, tiled=True)
+    tok_rows = token_mixed.shape[0]
+    pooled = jnp.einsum(
+        "tgc,gcd->tgd",
+        token_mixed.reshape(tok_rows, GROUPS, GROUP_DIM),
+        pool_weight,
+        preferred_element_type=jnp.float32,
+    )
+    pooled = (
+        (pooled * pool_scale.reshape(GROUPS, GROUP_DIM)).astype(jnp.bfloat16).reshape(tok_rows, -1)
+    )
+    return pooled
 
 
 def layer_kernel(n_tp, cuts, row_ref, meta_ref, wg_ref, wu_ref, wd_ref, out_ref,
@@ -451,34 +591,11 @@
     n_sp = lax.axis_size("sp")
     n_tp = lax.axis_size("tp")
     seg_rows, channels = pool_input.shape
-    last_rows = pool_input[seg_rows - reach_back :]
-    before = passed_along(last_rows, "sp", 1)
-    extended = jnp.concatenate([before, pool_input], axis=0).astype(jnp.float32)
-    first_chan = lax.axis_index("tp") * channels
-    chan_group = (first_chan + lax.iota(jnp.int32, channels)) // GROUP_DIM
-    positions = lax.axis_index("sp") * seg_rows + lax.iota(jnp.int32, seg_rows)
-    window = jnp.zeros((channels,), jnp.int32)
-    for group_level, win_len in enumerate(pool_windows):
-        window = jnp.where(chan_group == group_level, win_len, window)
-    running = jnp.zeros((seg_rows, channels), jnp.float32)
-    window_sum = running
-    for offset in range(pool_windows[-1]):
-        running = running + extended[reach_back - offset : reach_back - offset + seg_rows]
-        if offset + 1 in pool_windows:
-            window_sum = jnp.where(window[None, :] == offset + 1, running, window_sum)
-    divisor = jnp.minimum(positions[:, None] + 1, window[None, :]).astype(jnp.float32)
-    mixed_rows = (window_sum / divisor - extended[reach_back:]).astype(jnp.bfloat16)
-    token_mixed = lax.all_to_all(mixed_rows, "tp", split_axis=0, concat_axis=1, tiled=True)
-    tok_rows = token_mixed.shape[0]
-    pooled = jnp.einsum(
-        "tgc,gcd->tgd",
-        token_mixed.reshape(tok_rows, GROUPS, GROUP_DIM),
-        pool_weight,
-        preferred_element_type=jnp.float32,
-    )
-    pooled = (
-        (pooled * pool_scale.reshape(GROUPS, GROUP_DIM)).astype(jnp.bfloat16).reshape(tok_rows, -1)
-    )
+    if n_sp == 4 and n_tp == GROUPS and channels == GROUP_DIM and seg_rows == n_tp * 128:
+        pooled = mixed_tokens(pool_input, pool_weight, pool_scale, n_tp)
+    else:
+        pooled = routed_pool(pool_input, pool_weight, pool_scale)
+    tok_rows = pooled.shape[0]
     mix_out = jnp.dot(pooled, out_weight, preferred_element_type=jnp.float32)
     residual = (resid_in.astype(jnp.float32) + rms_scale(mix_out, mix_gain)).astype(jnp.bfloat16)
     normed = rms_scale(residual.astype(jnp.float32), ffn_gain).astype(jnp.bfloat16)

time: 156 us -> 154 us (0.987)
  Pallas kernels: 124 us -> 139 us
  starting transfers between devices: 8.2 us -> 0 us
  waiting for transfers between devices: 8.14 us -> 0 us
  matrix products: 3.24 us -> 5.69 us
    pallas_call x0 -> x1, Pallas kernels: none -> 14.2 us  [mixed_tokens(): pl.pallas_call(functools.partial(exchange_kernel, n_tp), out_shape=jax.Sh...]
    all_to_all x1 -> x0, waiting for transfers between devices: 8.14 us -> none  [per_device(): lax.all_to_all(mixed_rows, 'tp', split_axis=0, concat_axis=1, tiled=True)]
    all_to_all x1 -> x0, starting transfers between devices: 5.82 us -> none  [per_device(): lax.all_to_all(mixed_rows, 'tp', split_axis=0, concat_axis=1, tiled=True)]
    dot_general x1 -> x4, matrix products: 0.23 us -> 4.87 us  [mixed_tokens(): jnp.dot(mixed, pool_weight[group], preferred_element_type=jnp.float32)]
    ppermute x1 -> x0, starting transfers between devices: 2.38 us -> none  [passed_along(): return lax.ppermute(x, axis, pairs)]
    dot_general x1, matrix products: 3.01 us -> 0.82 us  [per_device(): mix_out = jnp.dot(pooled, out_weight, preferred_element_type=jnp.float32)]
  transfers between devices with their start and end apart: 2 -> 0, of which waited for: 1 -> 0; matrix products, arithmetic and copies ran while one was open for 2% -> 0% of each run, Pallas kernels for 0% -> 0%
where the time goes in v4:
time: 154 us
  Pallas kernels  139 us (90%)
  other arithmetic  7.16 us (5%)
  matrix products  5.69 us (4%)
  local copies, waits for them, and re-layouts  1.81 us (1%)
    pallas_call x1, Pallas kernels, dense_experts(): pl.pallas_call(functools.partial(layer_kernel, n_tp, cuts), out_shape=jax...  125 us
    pallas_call x1, Pallas kernels, mixed_tokens(): pl.pallas_call(functools.partial(exchange_kernel, n_tp), out_shape=jax.Sh...  14.2 us
    dot_general x4, matrix products, mixed_tokens(): jnp.dot(mixed, pool_weight[group], preferred_element_type=jnp.float32)  4.87 us

profile of v4, /device:TPU:0, one launch (start us, length us, event | category | flops | bytes accessed | tf_op | source)
XLA Modules:
  0.0 153.8 jit_solution(17904005554793119794)
XLA Ops:
  0.0 14.2 %pool_exchange.1 = bf16[4,144,256]{2,1,0:T(8,128)(2,1)} custom-call(bf16[512,256]{1,0:T(8,128)(2,1)} %pool_ref.1), custom_call_target="tpu_custom_call" | custom-call | tf_op jit(solution)/shard_map/pool_exchange/pallas_call | solution.py:131
  14.2 1.0 slice_convert_fusion.3
  15.2 0.0 copy-start
  15.2 0.9 fusion.74
  16.1 1.3 fusion
  17.4 1.1 fusion.1
  18.6 1.2 fusion.2
  19.7 0.0 copy-start.1
  19.7 0.0 copy-start.2
  19.7 1.3 fusion.3
  21.0 0.0 copy-done
  21.0 0.0 copy-start.3
  21.0 0.0 copy-start.5
  21.0 0.0 copy-start.6
  21.0 0.8 multiply_reduce_fusion
  21.9 0.0 copy-done.1
  21.9 0.0 copy-done.2
  21.9 0.4 fusion.6
  22.3 0.0 copy-done.3
  22.3 1.0 fusion.8.row_ref
  23.3 0.0 copy-done.5
  23.3 0.1 copy.14
  23.4 0.1 eq.29
  23.5 0.6 reduce-window.6
  24.1 0.2 slice_reduce_fusion
  24.4 0.1 eq.25
  24.5 0.1 fusion.71
  24.6 0.1 reshape.112
  24.8 0.1 copy.17
  24.8 0.1 pad.2.clone
  24.9 0.0 copy-done.6
  24.9 0.7 maximum_bitcast_fusion.meta_ref
  25.6 0.0 copy-start.4
  25.6 124.9 %routed_experts.1 = bf16[128,2048]{1,0:T(8,128)(2,1)} custom-call(bf16[128,2048]{1,0:T(8,128)(2,1)} %fusion.8.row_ref, f32[8,128]{1,0:T(8,128)} %maximum_bitcast_fusion.meta_ref, bf16[8,2048,256]{2,1,0:T(8,128)(2,1)} %wg_ref.1, bf16[8,2048,256]{2,1,0:T(8,128)(2,1)} %wu_ref.1, bf16[8,256,2048]{2,1,0:T(8,128)(2,1)} %wd_ref.1), custom_call_target="tpu_custom_call" | custom-call | tf_op jit(solution)/shard_map/routed_experts/pallas_call | solution.py:533
  150.5 1.2 fusion.4
  151.7 0.0 copy-done.4
  151.7 2.1 %fusion.9 = bf16[128,2048]{1,0:T(8,128)(2,1)} fusion(bf16[128,2048]{1,0:T(8,128)(2,1)} %routed_experts.1, bf16[128,2048]{1,0:T(8,128)(2,1)S(1)} %get-tuple-element.6, f32[2048]{0:T(1024)S(1)} %copy-done.4, f32[128]{0:T(128)S(1)} %add_rsqrt_fusion), kind=kLoop, calls=%fused_computation.18 | loop fusion | flops 1572864 | bytes 1581568 | tf_op jit(solution)/shard_map/convert_element_type | solution.py:605
  (10 shorter events, 0.1 us)
Async XLA Ops:
  15.2 5.8 %copy-start = (bf16[1024,2048]{1,0:T(8,128)(2,1)S(1)}, bf16[1024,2048]{1,0:T(8,128)(2,1)}, u32[]{:S(2)}) copy-start(bf16[1024,2048]{1,0:T(8,128)(2,1)} %param.17) | copy-start | bytes 12582916
  19.7 2.2 %copy-start.1 = (bf16[128,2048]{1,0:T(8,128)(2,1)S(1)}, bf16[128,2048]{1,0:T(8,128)(2,1)}, u32[]{:S(2)}) copy-start(bf16[128,2048]{1,0:T(8,128)(2,1)} %param.13) | copy-start | bytes 1572868
  19.7 2.2 %copy-start.2 = (f32[2048]{0:T(1024)S(1)}, f32[2048]{0:T(1024)}, u32[]{:S(2)}) copy-start(f32[2048]{0:T(1024)} %param.18) | copy-start | bytes 24580
  21.0 1.3 copy-start.3
  21.0 2.3 %copy-start.5 = (s32[128,2]{0,1:T(2,128)S(1)}, s32[128,2]{0,1:T(2,128)}, u32[]{:S(2)}) copy-start(s32[128,2]{0,1:T(2,128)} %param.23) | copy-start | bytes 3076
  21.0 3.9 %copy-start.6 = (f32[128,2]{0,1:T(2,128)S(1)}, f32[128,2]{0,1:T(2,128)}, u32[]{:S(2)}) copy-start(f32[128,2]{0,1:T(2,128)} %param.24) | copy-start | bytes 3076
  25.6 126.1 %copy-start.4 = (f32[2048]{0:T(1024)S(1)}, f32[2048]{0:T(1024)}, u32[]{:S(2)}) copy-start(f32[2048]{0:T(1024)} %param.25) | copy-start | bytes 24580

commit v5 on v4

--- a/solution.py
+++ b/solution.py
@@ -200,7 +200,7 @@
     tok, width = row_ref.shape
     local_experts, buffers = wg_ref.shape[0], wg.shape[0]
     slots = local_experts * SLOT
-    chunk = min(512, width)
+    chunk = min(1024, width)
     others = [(a, b) for a in range(4) for b in range(n_tp) if (a, b) != (0, 0)]
 
     def weight_copies(e):

time: 154 us -> 147 us (0.955)
  Pallas kernels: 139 us -> 131 us
    pallas_call x1, Pallas kernels: 125 us -> 117 us  [dense_experts(): pl.pallas_call(functools.partial(layer_kernel, n_tp, cuts), out_shape=jax...]
where the time goes in v5:
time: 147 us; the launch traced here: 146 us
  Pallas kernels  131 us (89%)
  other arithmetic  7.16 us (5%)
  matrix products  5.69 us (4%)
  local copies, waits for them, and re-layouts  1.81 us (1%)
    pallas_call x1, Pallas kernels, dense_experts(): pl.pallas_call(functools.partial(layer_kernel, n_tp, cuts), out_shape=jax...  117 us
    pallas_call x1, Pallas kernels, mixed_tokens(): pl.pallas_call(functools.partial(exchange_kernel, n_tp), out_shape=jax.Sh...  14.2 us
    dot_general x4, matrix products, mixed_tokens(): jnp.dot(mixed, pool_weight[group], preferred_element_type=jnp.float32)  4.87 us

profile of v5, /device:TPU:0, one launch (start us, length us, event | category | flops | bytes accessed | tf_op | source)
XLA Modules:
  0.0 146.3 jit_solution(9055374887555692229)
XLA Ops:
  0.0 14.2 %pool_exchange.1 = bf16[4,144,256]{2,1,0:T(8,128)(2,1)} custom-call(bf16[512,256]{1,0:T(8,128)(2,1)} %pool_ref.1), custom_call_target="tpu_custom_call" | custom-call | tf_op jit(solution)/shard_map/pool_exchange/pallas_call | solution.py:131
  14.2 1.0 slice_convert_fusion.3
  15.2 0.0 copy-start
  15.2 0.9 fusion.74
  16.1 1.3 fusion
  17.4 1.1 fusion.1
  18.6 1.2 fusion.2
  19.7 0.0 copy-start.1
  19.7 0.0 copy-start.2
  19.7 1.3 fusion.3
  21.0 0.0 copy-done
  21.0 0.0 copy-start.3
  21.0 0.0 copy-start.5
  21.0 0.0 copy-start.6
  21.0 0.8 multiply_reduce_fusion
  21.9 0.0 copy-done.1
  21.9 0.0 copy-done.2
  21.9 0.4 fusion.6
  22.3 0.0 copy-done.3
  22.3 1.0 fusion.8.row_ref
  23.3 0.0 copy-done.5
  23.3 0.1 copy.14
  23.4 0.1 eq.29
  23.5 0.6 reduce-window.6
  24.1 0.2 slice_reduce_fusion
  24.4 0.1 eq.25
  24.5 0.1 fusion.71
  24.6 0.1 reshape.112
  24.8 0.1 copy.17
  24.8 0.1 pad.2.clone
  24.9 0.0 copy-done.6
  24.9 0.7 maximum_bitcast_fusion.meta_ref
  25.6 0.0 copy-start.4
  25.6 117.3 %routed_experts.1 = bf16[128,2048]{1,0:T(8,128)(2,1)} custom-call(bf16[128,2048]{1,0:T(8,128)(2,1)} %fusion.8.row_ref, f32[8,128]{1,0:T(8,128)} %maximum_bitcast_fusion.meta_ref, bf16[8,2048,256]{2,1,0:T(8,128)(2,1)} %wg_ref.1, bf16[8,2048,256]{2,1,0:T(8,128)(2,1)} %wu_ref.1, bf16[8,256,2048]{2,1,0:T(8,128)(2,1)} %wd_ref.1), custom_call_target="tpu_custom_call" | custom-call | tf_op jit(solution)/shard_map/routed_experts/pallas_call | solution.py:533
  142.9 1.2 fusion.4
  144.2 0.0 copy-done.4
  144.2 2.1 %fusion.9 = bf16[128,2048]{1,0:T(8,128)(2,1)} fusion(bf16[128,2048]{1,0:T(8,128)(2,1)} %routed_experts.1, bf16[128,2048]{1,0:T(8,128)(2,1)S(1)} %get-tuple-element.6, f32[2048]{0:T(1024)S(1)} %copy-done.4, f32[128]{0:T(128)S(1)} %add_rsqrt_fusion), kind=kLoop, calls=%fused_computation.18 | loop fusion | flops 1572864 | bytes 1581568 | tf_op jit(solution)/shard_map/convert_element_type | solution.py:605
  (10 shorter events, 0.1 us)
Async XLA Ops:
  15.2 5.8 %copy-start = (bf16[1024,2048]{1,0:T(8,128)(2,1)S(1)}, bf16[1024,2048]{1,0:T(8,128)(2,1)}, u32[]{:S(2)}) copy-start(bf16[1024,2048]{1,0:T(8,128)(2,1)} %param.17) | copy-start | bytes 12582916
  19.7 2.2 %copy-start.1 = (bf16[128,2048]{1,0:T(8,128)(2,1)S(1)}, bf16[128,2048]{1,0:T(8,128)(2,1)}, u32[]{:S(2)}) copy-start(bf16[128,2048]{1,0:T(8,128)(2,1)} %param.13) | copy-start | bytes 1572868
  19.7 2.2 %copy-start.2 = (f32[2048]{0:T(1024)S(1)}, f32[2048]{0:T(1024)}, u32[]{:S(2)}) copy-start(f32[2048]{0:T(1024)} %param.18) | copy-start | bytes 24580
  21.0 1.3 copy-start.3
  21.0 2.3 %copy-start.5 = (s32[128,2]{0,1:T(2,128)S(1)}, s32[128,2]{0,1:T(2,128)}, u32[]{:S(2)}) copy-start(s32[128,2]{0,1:T(2,128)} %param.23) | copy-start | bytes 3076
  21.0 3.9 %copy-start.6 = (f32[128,2]{0,1:T(2,128)S(1)}, f32[128,2]{0,1:T(2,128)}, u32[]{:S(2)}) copy-start(f32[128,2]{0,1:T(2,128)} %param.24) | copy-start | bytes 3076
  25.6 118.6 %copy-start.4 = (f32[2048]{0:T(1024)S(1)}, f32[2048]{0:T(1024)}, u32[]{:S(2)}) copy-start(f32[2048]{0:T(1024)} %param.25) | copy-start | bytes 24580
